TPU v7x, 32 devices: a whole 2x2x4 slice. The times are simulated.
32 devices in a mesh: sp: 16 (over z, y, x), tp: 2 (over core).
Axes of the slice: x: 2, y: 2, z: 4, core: 2. Of those that a mesh axis runs over, the one named last changes fastest.
Arguments:
- resid: bfloat16 [2048, 2048], P('sp'), may hold values from -6 to 6
- queries: bfloat16 [2048, 1024], P('sp', 'tp'), may hold values from -6 to 6
- keys: bfloat16 [2048, 1024], P('sp', 'tp'), may hold values from -6 to 6
- values: bfloat16 [2048, 2048], P('sp', 'tp'), may hold values from -6 to 6
- decay_pre: float32 [2048, 1024], P('sp', 'tp'), may hold values from -4 to 11.5
- out_gate: bfloat16 [2048, 2048], P('sp', 'tp'), may hold values from -6 to 6
- head_gain: float32 [256], replicated, may hold values from 0.1 to 1.9
- out_proj: bfloat16 [2048, 2048], P('tp'), may hold values from -0.25 to 0.25
- mix_gain: float32 [2048], replicated, may hold values from 0.1 to 1.9
- mix_shift: float32 [2048], replicated, may hold values from -3 to 3
- gate_in: bfloat16 [2048, 5632], P('sp', 'tp'), may hold values from -0.125 to 0.125
- up_in: bfloat16 [2048, 5632], P('sp', 'tp'), may hold values from -0.125 to 0.125
- down_out: bfloat16 [5632, 2048], P('tp', 'sp'), may hold values from -0.25 to 0.25
- out_gain: float32 [2048], replicated, may hold values from 0.1 to 1.9
- out_shift: float32 [2048], replicated, may hold values from -2 to 2
Outputs:
- result: bfloat16 [2048, 2048], P('sp')
All inputs are finite; a program needn't handle non-finite values.
Results may differ from a plain program's by a relative error of at most 0.02.
Values may be sent and summed in bfloat16 or wider, within the bound.
A program may use at most 128 MiB of HBM per device.

v0:
```python
import functools

import jax
import jax.numpy as jnp
from jax import lax
from jax.experimental import pallas as pl
from jax.experimental.pallas import tpu as pltpu
from jax.sharding import PartitionSpec as P

HK = 128
HV = 256
SPAN = 64


ALPHA = 2.0**0.25
LN_EPS = 1e-05
RMS_EPS = 1e-06
TAU = 16.0
MESH = pl.DeviceIdType.MESH


def entering(array, axis, combine, identity):
    count, place = (lax.axis_size(axis), lax.axis_index(axis))
    everything = jax.tree.map(
        lambda part, kind: lax.all_gather(part.astype(kind), axis),
        array,
        (jnp.bfloat16, jnp.bfloat16),
    )
    start = jax.tree.map(
        lambda part, zero: jnp.broadcast_to(jnp.asarray(zero, part.dtype), part.shape),
        array,
        identity,
    )

    def lap(k, before):
        reached = k < place
        new = combine(
            before, jax.tree.map(lambda part, own: part[k].astype(own.dtype), everything, array)
        )
        return jax.tree.map(lambda a, b: jnp.where(reached, a, b), new, before)

    return lax.fori_loop(0, count, lap, start)


def layer_norm(inputs, gain, shift):
    center = inputs - jnp.mean(inputs, axis=-1, keepdims=True)
    spread = jnp.mean(center * center, axis=-1, keepdims=True)
    return center * lax.rsqrt(spread + LN_EPS) * gain + shift


def combine_states(earlier, later):
    return (earlier[0] * later[0], later[0][..., None] * earlier[1] + later[1])


def packed_state(own_decay, own_state):
    count = lax.axis_size("sp")
    rows, width = own_decay.size, own_state.shape[-1]
    decay = own_decay.reshape(count, rows // count, 1)
    high = decay.astype(jnp.bfloat16)
    low = (decay - high.astype(jnp.float32)).astype(jnp.bfloat16)
    fill = jnp.zeros((count, rows // count, 126), jnp.bfloat16)
    return jnp.concatenate(
        [own_state.reshape(count, rows // count, width).astype(jnp.bfloat16), high, low, fill],
        axis=-1,
    )


def greet(places):
    barrier = pltpu.get_barrier_semaphore()
    for place in places:
        pl.semaphore_signal(barrier, inc=1, device_id=place, device_id_type=MESH)
    pl.semaphore_wait(barrier, len(places))


def remote(src, dst, send, recv, place):
    return pltpu.make_async_remote_copy(
        src_ref=src, dst_ref=dst, send_sem=send, recv_sem=recv, device_id=place, device_id_type=MESH
    )


def local_tokens(queries, keys, values, decay_pre):
    tok_rows = queries.shape[0]
    local_heads = queries.shape[1] // HK
    blocks = tok_rows // SPAN
    logdecay = jax.nn.log_sigmoid(decay_pre) / TAU
    scaled_q = queries.astype(jnp.float32).reshape(blocks, SPAN, local_heads, HK) * HK ** (-0.5)
    key_block = keys.astype(jnp.float32).reshape(blocks, SPAN, local_heads, HK)
    value_block = values.astype(jnp.float32).reshape(blocks, SPAN, local_heads, HV)
    cumul = jnp.cumsum(logdecay.reshape(blocks, SPAN, local_heads, HK), axis=1)
    last = cumul[:, -1]
    key_decayed = key_block * jnp.exp(last[:, None] - cumul)
    updates = jnp.einsum(
        "nchk,nchv->nhkv", key_decayed, value_block, precision=lax.Precision.HIGHEST
    )

    def advance(running_state, inputs):
        decay_end, state_increment, current_query = inputs
        running_state = jnp.exp(decay_end)[..., None] * running_state + state_increment
        return (
            running_state,
            jnp.einsum(
                "qpy,pyr->qpr", current_query, running_state, precision=lax.Precision.HIGHEST
            ),
        )

    own_state, local_read = lax.scan(
        advance, jnp.zeros((local_heads, HK, HV), jnp.float32), (last, updates, scaled_q)
    )
    block_ends = jnp.cumsum(last, axis=0)
    own_decay = jnp.exp(block_ends[-1])
    carry_q = scaled_q * jnp.exp(block_ends)[:, None]
    return local_read, carry_q, own_decay, own_state


def mix_tokens(local_read, carry_q, own_decay, own_state, out_gate, head_gain):
    blocks, span, local_heads, _ = carry_q.shape
    tok_rows = blocks * span
    identity = (jnp.ones_like(own_decay), jnp.zeros_like(own_state))
    _, incoming = entering((own_decay, own_state), "sp", combine_states, identity)
    carried = jnp.einsum(
        "xepj,pjw->xepw", carry_q, incoming, precision=lax.Precision.HIGHEST
    )
    state_readout = (local_read + carried).reshape(tok_rows, local_heads, HV)
    normed = (
        state_readout
        * lax.rsqrt(jnp.mean(state_readout * state_readout, axis=-1, keepdims=True) + RMS_EPS)
        * head_gain
    )
    return (
        normed.reshape(tok_rows, local_heads * HV) * jax.nn.silu(out_gate.astype(jnp.float32))
    ).astype(jnp.bfloat16)


def hidden_by_rows(whole_rows, gate_in, up_in):
    gate = jnp.dot(
        whole_rows,
        lax.all_gather(gate_in, "sp", axis=0, tiled=True),
        preferred_element_type=jnp.float32,
    )
    upward = jnp.dot(
        whole_rows,
        lax.all_gather(up_in, "sp", axis=0, tiled=True),
        preferred_element_type=jnp.float32,
    )
    return (jax.nn.silu(gate) * upward).astype(jnp.bfloat16)


def down_by_columns(hidden, down_out):
    return jnp.dot(
        hidden,
        lax.all_gather(down_out, "sp", axis=1, tiled=True),
        preferred_element_type=jnp.float32,
    )


def own_units(gate_in, up_in, down_out):
    count = lax.axis_size("sp")
    inner, units = gate_in.shape
    piece = units // count
    sent = jnp.concatenate(
        [
            gate_in.T.reshape(count, piece, inner),
            up_in.T.reshape(count, piece, inner),
            down_out.reshape(count, piece, inner),
        ],
        axis=1,
    )
    return sent


def layer_kernel(
    count,
    width,
    states,
    local_read,
    carry_q,
    out_gate,
    head_gain,
    out_proj,
    resid,
    mix_gain,
    mix_shift,
    sent,
    gain,
    shift,
    out,
    got,
    starts,
    back,
    proj,
    gated,
    mixed,
    mixed_in,
    mid,
    rows,
    weights,
    part,
    twin_in,
    b_out,
    b_in,
    a_out,
    a_in,
    z_out,
    z_in,
    send1,
    recv1,
    send2,
    recv2,
    m_sem,
    w_send,
    w_recv,
    g_send,
    g_recv,
    t_recv,
    own_sem,
    s_send,
    p_send,
    p_recv,
    b_recv,
    a_recv,
    z_recv,
    f_sem,
):
    me, core = lax.axis_index("sp"), lax.axis_index("tp")
    deep = count // 4
    own, inner = mid.shape
    piece = sent.shape[1] // 3
    lanes = sent.shape[2]
    x, y = me % 2, (me // 2) % 2
    to_x, to_y = 1 - 2 * x, 2 - 4 * y
    to_a = (1 - core) * to_y + core * to_x
    to_b = core * to_y + (1 - core) * to_x
    place_a, place_b = (me + to_a, core), (me + to_b, core)
    twin = (me, 1 - core)
    others = [((me + j) % count, core) for j in range(1, count)]

    def spot(k, a, b):
        return (me + 4 * k) % count + a * to_a + b * to_b

    greet(others + [twin])

    moved = []
    for j, place in enumerate(others, 1):
        copy = remote(states.at[place[0]], got.at[me], send1.at[j], recv1.at[j], place)
        copy.start()
        moved.append(copy)
    columns = pl.ds(pl.multiple_of(me * lanes, lanes), lanes)
    keep = [
        pltpu.make_async_copy(states.at[me], got.at[me], own_sem.at[0]),
        pltpu.make_async_copy(out_proj, proj, own_sem.at[1]),
        pltpu.make_async_copy(sent.at[me], weights.at[:, columns], own_sem.at[2]),
    ]
    for copy in keep:
        copy.start()
    keep[0].wait()
    for copy in moved:
        copy.wait_recv()
    running = jnp.zeros(starts.shape[1:], jnp.float32)
    for k in range(count):
        starts[k] = running.astype(starts.dtype)
        if k < count - 1:
            state = got[k].astype(jnp.float32)
            decay = state[:, width : width + 1] + state[:, width + 1 : width + 2]
            running = decay * running + state[:, :width]
    returned = []
    for j, place in enumerate(others, 1):
        copy = remote(starts.at[place[0]], back.at[me], send2.at[j], recv2.at[j], place)
        copy.start()
        returned.append(copy)
    mine = pltpu.make_async_copy(starts.at[me], back.at[me], own_sem.at[3])
    mine.start()
    brought = []

    def bring(first, last):
        taken = pl.ds(first * piece, (last - first) * piece)
        for place in others:
            slot = len(brought)
            copy = remote(
                sent.at[place[0], taken],
                weights.at[taken, columns],
                w_send.at[slot],
                w_recv.at[slot],
                place,
            )
            copy.start()
            brought.append(copy)

    bring(0, 1)
    mine.wait()
    for copy in returned:
        copy.wait_recv()

    heads = gated.shape[1] // width
    key_width = carry_q.shape[1] // heads
    each = count // heads
    for h in range(heads):
        wide = slice(h * width, (h + 1) * width)
        incoming = back[h * each : (h + 1) * each].reshape(key_width, width).astype(jnp.float32)
        read = local_read[:, wide] + jnp.dot(
            carry_q[:, h * key_width : (h + 1) * key_width],
            incoming,
            precision=lax.Precision.HIGHEST,
            preferred_element_type=jnp.float32,
        )
        size = jnp.mean(read * read, axis=-1, keepdims=True)
        pre = out_gate[:, wide].astype(jnp.float32)
        normed = read * lax.rsqrt(size + RMS_EPS) * head_gain[...]
        gated[:, wide] = (normed * (pre * jax.nn.sigmoid(pre))).astype(jnp.bfloat16)
    keep[1].wait()
    summed_heads = jnp.dot(gated[...], proj[...], preferred_element_type=jnp.float32)
    mixed[...] = summed_heads.astype(jnp.bfloat16).reshape(2, own, inner)
    swap = remote(mixed.at[1 - core], mixed_in, m_sem.at[0], m_sem.at[1], twin)
    swap.start()
    swap.wait()
    total = mixed[core].astype(jnp.float32) + mixed_in[...].astype(jnp.float32)
    before = ALPHA * resid[core].astype(jnp.float32) + total
    middle = layer_norm(before, mix_gain[...], mix_shift[...]).astype(jnp.bfloat16)
    mid[...] = middle
    rows[2 * me + core] = middle

    sends = []

    def forward(k, a, b, place, slot, recv):
        block = 2 * spot(k, a, b) + core
        src = mid if (k, a, b) == (0, 0, 0) else rows.at[block]
        copy = remote(src, rows.at[block], g_send.at[len(sends)], recv.at[slot], place)
        copy.start()
        sends.append(copy)

    def index(k, a, b):
        return (k * 2 + a) * 2 + b

    def landed(k, a, b):
        block = rows.at[2 * spot(k, a, b) + core]
        remote(block, block, g_send.at[0], g_recv.at[index(k, a, b)], twin).wait_recv()

    def onward(k, a, b):
        if not b:
            if not a:
                forward(k, 0, 0, place_a, index(k, 1, 0), g_recv)
            forward(k, a, 0, place_b, index(k, a, 1), g_recv)
        forward(k, a, b, twin, index(k, b, a), t_recv)

    for k in range(1, deep):
        forward(0, 0, 0, ((me + 4 * k) % count, core), index(deep - k, 0, 0), g_recv)
    onward(0, 0, 0)
    bring(1, 2)
    order = [(0, 1, 0)] + [(k, 0, 0) for k in range(1, deep)]
    order += [(k, 1, 0) for k in range(1, deep)]
    order += [(k, a, 1) for k in range(deep) for a in range(2)]
    for block in order:
        landed(*block)
        onward(*block)
        if block == (deep - 1, 0, 0):
            bring(2, 3)
    for k in range(deep):
        for a in range(2):
            for b in range(2):
                block = rows.at[2 * spot(k, b, a) + 1 - core]
                remote(block, block, g_send.at[0], t_recv.at[index(k, a, b)], twin).wait_recv()
    keep[2].wait()
    for copy in brought:
        copy.wait_recv()
    for copy in sends + moved + returned + brought:
        copy.wait_send()

    contract = (((1,), (1,)), ((), ()))

    def to_twin(place):
        return remote(
            part.at[2 * place + 1 - core],
            twin_in.at[place],
            p_send.at[place],
            p_recv.at[place],
            twin,
        )

    def tile(step, side):
        i = 2 * ((me // 4 + step) % deep) + side
        left = rows[pl.ds(4 * i, 4)].reshape(4 * own, inner)
        gate = lax.dot_general(left, weights[:piece], contract, preferred_element_type=jnp.float32)
        up = lax.dot_general(
            left, weights[piece : 2 * piece], contract, preferred_element_type=jnp.float32
        )
        hidden = (gate * jax.nn.sigmoid(gate) * up).astype(jnp.bfloat16)
        down = jnp.dot(hidden, weights[2 * piece :], preferred_element_type=jnp.float32)
        part[pl.ds(4 * i, 4)] = down.astype(jnp.bfloat16).reshape(4, own, inner)
        to_twin(2 * i).start()
        to_twin(2 * i + 1).start()
        return side

    def summed(k, a, b, arrived):
        place = spot(k, a, b)
        to_twin(place).wait_recv()
        total = part[2 * place + core].astype(jnp.float32) + twin_in[place].astype(jnp.float32)
        for ref, sem, slot in arrived:
            remote(ref.at[slot], ref.at[slot], s_send.at[0], sem.at[slot], twin).wait_recv()
            total = total + ref[slot].astype(jnp.float32)
        return total

    pushed = []

    def push(src, dst, recv, slot, place):
        copy = remote(src.at[slot], dst.at[slot], s_send.at[len(pushed)], recv.at[slot], place)
        copy.start()
        pushed.append(copy)

    turn = [k for k in range(1, deep)] + [0]
    for a in (1, 0):
        lax.fori_loop(0, deep, tile, a * (1 - y) + (1 - a) * y)
        for k in turn:
            slot = 2 * k + a
            b_out[slot] = summed(k, a, 1, []).astype(jnp.bfloat16)
            push(b_out, b_in, b_recv, slot, place_b)
    for k in turn:
        a_out[k] = summed(k, 1, 0, [(b_in, b_recv, 2 * k + 1)]).astype(jnp.bfloat16)
        push(a_out, a_in, a_recv, k, place_a)
    for k in range(1, deep):
        z_out[k] = summed(k, 0, 0, [(b_in, b_recv, 2 * k), (a_in, a_recv, k)]).astype(jnp.bfloat16)
        push(z_out, z_in, z_recv, k, ((me + 4 * k) % count, core))
    arrived = [(b_in, b_recv, 0), (a_in, a_recv, 0)] + [(z_in, z_recv, k) for k in range(1, deep)]
    ffn = summed(0, 0, 0, arrived)
    finished = layer_norm(
        ALPHA * mid[...].astype(jnp.float32) + 0.5 * ffn, gain[...], shift[...]
    )
    out[core] = finished.astype(jnp.bfloat16)
    last = remote(out.at[core], out.at[core], f_sem.at[0], f_sem.at[1], twin)
    last.start()

    def drained(place, carry):
        to_twin(place).wait_send()
        return carry

    lax.fori_loop(0, count, drained, 0)
    for copy in pushed:
        copy.wait_send()
    last.wait()


def layer(local, out_gate, head_gain, out_proj, resid, mix_gain, mix_shift, sent, gain, shift):
    local_read, carry_q, own_decay, own_state = local
    count = lax.axis_size("sp")
    tok_rows, inner = resid.shape
    own = tok_rows // 2
    deep = count // 4
    states = packed_state(own_decay, own_state)
    _, slice_rows, wide = states.shape
    width = own_state.shape[-1]
    dma = pltpu.SemaphoreType.DMA
    block = lambda *lead: pltpu.VMEM((*lead, own, inner), jnp.bfloat16)
    near, far = pl.BlockSpec(memory_space=pltpu.VMEM), pl.BlockSpec(memory_space=pl.ANY)
    out = pl.pallas_call(
        functools.partial(layer_kernel, count, width),
        out_shape=jax.ShapeDtypeStruct((2, own, inner), jnp.bfloat16),
        in_specs=[near] * 5 + [far] + [near] * 3 + [far] + [near] * 2,
        out_specs=near,
        scratch_shapes=[
            pltpu.VMEM((count, slice_rows, wide), jnp.bfloat16),
            pltpu.VMEM((count, slice_rows, width), jnp.bfloat16),
            pltpu.VMEM((count, slice_rows, width), jnp.bfloat16),
            pltpu.VMEM(out_proj.shape, jnp.bfloat16),
            pltpu.VMEM((tok_rows, out_proj.shape[0]), jnp.bfloat16),
            block(2),
            block(),
            block(),
            block(2 * count),
            pltpu.VMEM((sent.shape[1], inner), jnp.bfloat16),
            block(2 * count),
            block(count),
            block(2 * deep),
            block(2 * deep),
            block(deep),
            block(deep),
            block(deep),
            block(deep),
            dma((count,)),
            dma((count,)),
            dma((count,)),
            dma((count,)),
            dma((2,)),
            dma((3 * count,)),
            dma((3 * count,)),
            dma((2 * count,)),
            dma((count,)),
            dma((count,)),
            dma((4,)),
            dma((count,)),
            dma((count,)),
            dma((count,)),
            dma((2 * deep,)),
            dma((deep,)),
            dma((deep,)),
            dma((2,)),
        ],
        compiler_params=pltpu.CompilerParams(
            collective_id=2, has_side_effects=True, vmem_limit_bytes=60 * 1024 * 1024
        ),
    )(
        states,
        local_read.reshape(tok_rows, -1),
        carry_q.reshape(tok_rows, -1),
        out_gate,
        head_gain[None],
        out_proj,
        resid.reshape(2, own, inner),
        mix_gain[None],
        mix_shift[None],
        sent,
        gain[None],
        shift[None],
    )
    return out.reshape(tok_rows, inner)


def body(
    resid,
    queries,
    keys,
    values,
    decay_pre,
    out_gate,
    head_gain,
    out_proj,
    mix_gain,
    mix_shift,
    gate_in,
    up_in,
    down_out,
    out_gain,
    out_shift,
):
    tp_count = lax.axis_size("tp")
    tok_rows = queries.shape[0]
    own_count = tok_rows // tp_count
    sp_count = lax.axis_size("sp")
    units = gate_in.shape[1]
    key_rows, heads = queries.shape[1], queries.shape[1] // HK
    by_units = (
        2 * tok_rows * sp_count < 3 * units
        and units % sp_count == 0
        and (units // sp_count) % 16 == 0
        and gate_in.shape[0] == down_out.shape[1]
        and tp_count == 2
        and sp_count % 4 == 0
        and own_count % 16 == 0
        and key_rows % (16 * sp_count) == 0
        and sp_count % heads == 0
    )
    local = local_tokens(queries, keys, values, decay_pre)
    if by_units:
        sent = own_units(gate_in, up_in, down_out)
        norms = (mix_gain, mix_shift, sent, out_gain, out_shift)
        return layer(local, out_gate, head_gain, out_proj, resid, *norms)
    gated = mix_tokens(*local, out_gate, head_gain)
    mixed = lax.psum_scatter(
        jnp.dot(gated, out_proj, preferred_element_type=jnp.float32).astype(jnp.bfloat16),
        "tp",
        scatter_dimension=0,
        tiled=True,
    ).astype(jnp.float32)
    own_resid = lax.dynamic_slice_in_dim(resid, lax.axis_index("tp") * own_count, own_count, 0)
    mid = layer_norm(ALPHA * own_resid.astype(jnp.float32) + mixed, mix_gain, mix_shift).astype(
        jnp.bfloat16
    )
    whole_rows = lax.all_gather(mid, "tp", axis=0, tiled=True)
    hidden = hidden_by_rows(whole_rows, gate_in, up_in)
    ffn = lax.psum_scatter(
        down_by_columns(hidden, down_out).astype(jnp.bfloat16),
        "tp",
        scatter_dimension=0,
        tiled=True,
    ).astype(jnp.float32)
    finished = layer_norm(ALPHA * mid.astype(jnp.float32) + 0.5 * ffn, out_gain, out_shift).astype(
        jnp.bfloat16
    )
    return lax.all_gather(finished, "tp", axis=0, tiled=True)


def solution(mesh):
    return jax.shard_map(
        body,
        mesh=mesh,
        in_specs=(
            P("sp", None),
            P("sp", "tp"),
            P("sp", "tp"),
            P("sp", "tp"),
            P("sp", "tp"),
            P("sp", "tp"),
            P(),
            P("tp", None),
            P(),
            P(),
            P("sp", "tp"),
            P("sp", "tp"),
            P("tp", "sp"),
            P(),
            P(),
        ),
        out_specs=P("sp", None),
        check_vma=False,
    )
```

profile of v0, /device:TPU:0, one launch (start us, length us, event | category | flops | bytes accessed | tf_op | source)
XLA Modules:
  0.0 171.0 jit_solution(14063099501469848316)
XLA Ops:
  0.0 0.1 pad.6.clone
  0.1 1.0 reshape.94
  1.1 1.1 reshape.86
  2.2 1.1 fusion.1
  3.3 0.1 reshape.83
  3.4 0.1 fusion.6
  3.5 0.1 exponential_multiply_fusion
  3.7 0.1 exp.48
  3.8 0.2 copy.35
  4.0 0.2 copy.33
  4.1 0.2 copy.34
  4.4 0.0 copy-done.3
  4.4 0.8 convert_multiply_fusion
  5.2 0.1 mul.38
  5.3 0.6 fusion.2
  5.9 0.0 copy-start
  5.9 3.1 %while.13 = (s32[]{:T(128)}, f32[4,128,256]{2,1,0:T(8,128)S(1)}, f32[2,64,4,256]{3,2,1,0:T(4,128)}, f32[2,4,128]{2,1,0:T(4,128)S(1)}, f32[2,4,128,256]{3,2,1,0:T...) while((s32[]{:T(128)}, f32[4,128,256]{2,1,0:T(8,128)S(1)}, ...), condition=%wide.region_2.3_spmd.clone, body=%wide.region_1.2_spmd.clone.sunk | while | flops 101056512 | bytes 3283063 | solution.py:106
  6.0 0.2 bitcast_add_fusion.2
  6.2 0.4 convolution_bitcast_fusion.2
  6.6 0.9 copy_dynamic-update-slice_fusion.2
  7.5 0.2 bitcast_add_fusion.2
  7.7 0.4 convolution_bitcast_fusion.2
  8.2 0.9 copy_dynamic-update-slice_fusion.2
  9.1 2.0 %copy.44 = f32[16,8,4,256]{3,1,2,0:T(8,128)} copy(f32[16,8,4,256]{3,2,1,0:T(4,128)} %bitcast.21) | data formatting | bytes 1048576
  11.1 0.9 maximum_maximum_fusion.states
  12.0 0.0 copy-done
  12.0 0.3 copy.37
  12.4 0.0 copy-done.1
  12.4 0.3 copy.38
  12.7 1.5 pad_maximum_fusion.sent
  14.2 154.9 %shard_map.145 = bf16[2,64,2048]{2,1,0:T(8,128)(2,1)} custom-call(bf16[16,32,384]{2,1,0:T(8,128)(2,1)} %maximum_maximum_fusion.states, f32[128,1024]{1,0:T(8,128)} %bitcast.50, f32[128,512]{1,0:T(8,128)} %get-tuple-element.91.carry_q, bf16[128,1024]{1,0:T(8,128)(2,1)} %out_gate.1, f32[1,256]{1,0:T(1,128)} %bitcast.62, bf16[1024,2048]{1,0:T(8,128)(2,1)} %out_proj.1, ...), custom_call_target="tpu_custom_call" | custom-call | tf_op jit(solution)/shard_map/pallas_call | solution.py:452
  169.1 1.9 %copy.69 = bf16[128,2048]{1,0:T(8,128)(2,1)} copy(bf16[128,2048]{1,0:T(8,128)(2,1)} %bitcast.51) | data formatting | bytes 1048576
  (18 shorter events, 0.2 us)
Async XLA Ops:
  0.0 4.4 %copy-start.3 = (bf16[128,512]{1,0:T(8,128)(2,1)S(1)}, bf16[128,512]{1,0:T(8,128)(2,1)}, u32[]{:S(2)}) copy-start(bf16[128,512]{1,0:T(8,128)(2,1)} %param.18) | copy-start | bytes 393220
  5.9 6.1 %copy-start = (bf16[128,2816]{1,0:T(8,128)(2,1)S(1)}, bf16[128,2816]{1,0:T(8,128)(2,1)}, u32[]{:S(2)}) copy-start(bf16[128,2816]{1,0:T(8,128)(2,1)} %param.27) | copy-start | bytes 2162692
  9.1 3.3 %copy-start.1 = (bf16[128,2816]{1,0:T(8,128)(2,1)S(1)}, bf16[128,2816]{1,0:T(8,128)(2,1)}, u32[]{:S(2)}) copy-start(bf16[128,2816]{1,0:T(8,128)(2,1)} %param.28) | copy-start | bytes 2162692
  9.1 3.7 %copy-start.2 = (bf16[2816,128]{1,0:T(8,128)(2,1)S(1)}, bf16[2816,128]{1,0:T(8,128)(2,1)}, u32[]{:S(2)}) copy-start(bf16[2816,128]{1,0:T(8,128)(2,1)} %param.29) | copy-start | bytes 2162692
where the time goes:
time: 174 us; the launch traced here: 171 us
  Pallas kernels  155 us (89%)
  local copies, waits for them, and re-layouts  9.51 us (5%)
  other arithmetic  4.89 us (3%)
    pallas_call x1, Pallas kernels, layer(): pl.pallas_call(functools.partial(layer_kernel, count, width), out_shape=j...  155 us
    unnamed x10, local copies, waits for them, and re-layouts  3.94 us

commit v1 on v0

v1 whole, which is shorter than its diff:
```python
import functools

import jax
import jax.numpy as jnp
from jax import lax
from jax.experimental import pallas as pl
from jax.experimental.pallas import tpu as pltpu
from jax.sharding import PartitionSpec as P

HK = 128
HV = 256
SPAN = 64
LANES = 128


ALPHA = 2.0**0.25
LN_EPS = 1e-05
RMS_EPS = 1e-06
TAU = 16.0
MESH = pl.DeviceIdType.MESH


def entering(array, axis, combine, identity):
    count, place = (lax.axis_size(axis), lax.axis_index(axis))
    everything = jax.tree.map(
        lambda part, kind: lax.all_gather(part.astype(kind), axis),
        array,
        (jnp.bfloat16, jnp.bfloat16),
    )
    start = jax.tree.map(
        lambda part, zero: jnp.broadcast_to(jnp.asarray(zero, part.dtype), part.shape),
        array,
        identity,
    )

    def lap(k, before):
        reached = k < place
        new = combine(
            before, jax.tree.map(lambda part, own: part[k].astype(own.dtype), everything, array)
        )
        return jax.tree.map(lambda a, b: jnp.where(reached, a, b), new, before)

    return lax.fori_loop(0, count, lap, start)


def layer_norm(inputs, gain, shift):
    center = inputs - jnp.mean(inputs, axis=-1, keepdims=True)
    spread = jnp.mean(center * center, axis=-1, keepdims=True)
    return center * lax.rsqrt(spread + LN_EPS) * gain + shift


def combine_states(earlier, later):
    return (earlier[0] * later[0], later[0][..., None] * earlier[1] + later[1])


def greet(places):
    barrier = pltpu.get_barrier_semaphore()
    for place in places:
        pl.semaphore_signal(barrier, inc=1, device_id=place, device_id_type=MESH)
    pl.semaphore_wait(barrier, len(places))


def remote(src, dst, send, recv, place):
    return pltpu.make_async_remote_copy(
        src_ref=src, dst_ref=dst, send_sem=send, recv_sem=recv, device_id=place, device_id_type=MESH
    )


def local_tokens(queries, keys, values, decay_pre):
    tok_rows = queries.shape[0]
    local_heads = queries.shape[1] // HK
    blocks = tok_rows // SPAN
    logdecay = jax.nn.log_sigmoid(decay_pre) / TAU
    scaled_q = queries.astype(jnp.float32).reshape(blocks, SPAN, local_heads, HK) * HK ** (-0.5)
    key_block = keys.astype(jnp.float32).reshape(blocks, SPAN, local_heads, HK)
    value_block = values.astype(jnp.float32).reshape(blocks, SPAN, local_heads, HV)
    cumul = jnp.cumsum(logdecay.reshape(blocks, SPAN, local_heads, HK), axis=1)
    last = cumul[:, -1]
    key_decayed = key_block * jnp.exp(last[:, None] - cumul)
    updates = jnp.einsum(
        "nchk,nchv->nhkv", key_decayed, value_block, precision=lax.Precision.HIGHEST
    )

    def advance(running_state, inputs):
        decay_end, state_increment, current_query = inputs
        running_state = jnp.exp(decay_end)[..., None] * running_state + state_increment
        return (
            running_state,
            jnp.einsum(
                "qpy,pyr->qpr", current_query, running_state, precision=lax.Precision.HIGHEST
            ),
        )

    own_state, local_read = lax.scan(
        advance, jnp.zeros((local_heads, HK, HV), jnp.float32), (last, updates, scaled_q)
    )
    block_ends = jnp.cumsum(last, axis=0)
    own_decay = jnp.exp(block_ends[-1])
    carry_q = scaled_q * jnp.exp(block_ends)[:, None]
    return local_read, carry_q, own_decay, own_state


def mix_tokens(local_read, carry_q, own_decay, own_state, out_gate, head_gain):
    blocks, span, local_heads, _ = carry_q.shape
    tok_rows = blocks * span
    identity = (jnp.ones_like(own_decay), jnp.zeros_like(own_state))
    _, incoming = entering((own_decay, own_state), "sp", combine_states, identity)
    carried = jnp.einsum(
        "xepj,pjw->xepw", carry_q, incoming, precision=lax.Precision.HIGHEST
    )
    state_readout = (local_read + carried).reshape(tok_rows, local_heads, HV)
    normed = (
        state_readout
        * lax.rsqrt(jnp.mean(state_readout * state_readout, axis=-1, keepdims=True) + RMS_EPS)
        * head_gain
    )
    return (
        normed.reshape(tok_rows, local_heads * HV) * jax.nn.silu(out_gate.astype(jnp.float32))
    ).astype(jnp.bfloat16)


def hidden_by_rows(whole_rows, gate_in, up_in):
    gate = jnp.dot(
        whole_rows,
        lax.all_gather(gate_in, "sp", axis=0, tiled=True),
        preferred_element_type=jnp.float32,
    )
    upward = jnp.dot(
        whole_rows,
        lax.all_gather(up_in, "sp", axis=0, tiled=True),
        preferred_element_type=jnp.float32,
    )
    return (jax.nn.silu(gate) * upward).astype(jnp.bfloat16)


def down_by_columns(hidden, down_out):
    return jnp.dot(
        hidden,
        lax.all_gather(down_out, "sp", axis=1, tiled=True),
        preferred_element_type=jnp.float32,
    )


def layer_kernel(
    deep,
    wide,
    queries,
    keys,
    values,
    decay_pre,
    out_gate,
    head_gain,
    out_proj,
    resid,
    mix_gain,
    mix_shift,
    gate_in,
    up_in,
    down_out,
    gain,
    shift,
    out,
    w1,
    w2,
    proj,
    updates,
    ends,
    s_out,
    d_out,
    s_in,
    d_in,
    before,
    total,
    t_out,
    t_in,
    dt_out,
    dt_in,
    s_start,
    start,
    gated,
    mixed,
    mixed_in,
    rows,
    hidden,
    part,
    y_in,
    u_in,
    v_in,
    z_out,
    acc,
    own_sem,
    b_send,
    b_recv,
    f_send,
    f_recv,
    t_send,
    t_recv,
    p1_send,
    p1_recv,
    p2_send,
    p2_recv,
    p3_send,
    p3_recv,
    m_sem,
    au_send,
    av_send,
    ay_send,
    az_recv,
    ay_recv,
    ry_send,
    ry_recv,
    rz_send,
    ru_recv,
    rv_recv,
    f_sem,
):
    me, core = lax.axis_index("sp"), lax.axis_index("tp")
    x, y, z = me % 2, (me // 2) % 2, me // 4
    group = me // 2
    groups = 2 * deep
    plane = 4
    place = me % plane
    own, inner = rows.shape[2], rows.shape[3]
    depth = gate_in.shape[0]
    lanes = down_out.shape[1]
    span = wide * LANES
    half = lambda c: pl.ds(pl.multiple_of(c * span, span), span)
    twin = (me, 1 - core)
    x_place = (me + 1 - 2 * x, core)
    y_place = (me + 2 - 4 * y, core)
    above, below = (me + plane, core), (me - plane, core)
    sides = [(dy, dz) for dz in range(deep) for dy in range(2)]

    def at(xx, yy, zz):
        return (plane * zz + 2 * yy + xx, core)

    def target(r):
        dy, dz = sides[r]
        return (y + dy) % 2, (z + dz) % deep

    def origin(r):
        dy, dz = sides[r]
        return (y + dy) % 2, (z + deep - dz) % deep

    def fellow(dp):
        return (x + dp % 2) % 2, (y + dp // 2) % 2

    def short(c, g):
        return jnp.logical_or(g == c, g == groups - 2 + c)

    def first_block(c, g):
        return wide * g - (g > c).astype(jnp.int32) - (g > groups - 2 + c).astype(jnp.int32)

    def sized(flag, run):
        @pl.when(flag)
        def _():
            run(wide - 1)

        @pl.when(jnp.logical_not(flag))
        def _():
            run(wide)

    def taken(mat, g, blocks):
        begin = pl.ds(pl.multiple_of(first_block(core, g) * LANES, LANES), blocks * LANES)
        return (gate_in.at[:, begin], up_in.at[:, begin], down_out.at[begin])[mat]

    def landing(mat, c, s, blocks):
        if mat < 2:
            rows_of = pl.ds(pl.multiple_of(s * depth, depth), depth)
            return w1.at[c, rows_of, pl.ds(mat * span, blocks * LANES)]
        columns = pl.ds(pl.multiple_of(s * lanes, lanes), lanes)
        return w2.at[pl.ds(pl.multiple_of(c * span, span), blocks * LANES), columns]

    def slab(j, c, s):
        if j == 0:
            return w1.at[c, pl.ds(pl.multiple_of(s * depth, depth), depth)]
        return landing(2, c, s, wide)

    def bring(mat, r, run):
        yy, zz = target(r)
        goal = at(x, yy, zz) if r else x_place
        g = 2 * zz + yy

        def copy(blocks):
            run(
                remote(
                    taken(mat, g, blocks),
                    landing(mat, core, me, blocks),
                    b_send.at[mat, r],
                    b_recv.at[mat, r],
                    goal,
                )
            )

        sized(short(core, g), copy)

    def send(mat, *which):
        for r in which:
            bring(mat, r, lambda copy: copy.start())

    def relay(mat, r):
        yy, zz = origin(r)
        s = plane * zz + 2 * yy + x
        block = landing(mat, core, s, wide)
        return remote(block, block, f_send.at[mat, r], f_recv.at[mat, r], x_place)

    def share(j, k, r):
        yy, zz = origin(r)
        s = plane * zz + 2 * yy + (x + k) % 2
        block = slab(j, core, s)
        return remote(block, block, t_send.at[j, k, r], t_recv.at[j, k, r], twin)

    def came(ref, sem):
        remote(ref, ref, f_sem.at[0], sem, twin).wait_recv()

    def shared(mat, k, r):
        if mat:
            share(mat - 1, k, r).start()

    def pass_on(mat, *which):
        for r in which:
            yy, zz = origin(r)
            s = plane * zz + 2 * yy + x if r else x_place[0]
            sized(
                short(core, group),
                lambda blocks, s=s, r=r: came(landing(mat, core, s, blocks), b_recv.at[mat, r]),
            )
            if r:
                relay(mat, r).start()
            shared(mat, 0 if r else 1, r)

    def passed(mat, *which):
        for r in which:
            yy, zz = origin(r)
            came(landing(mat, core, plane * zz + 2 * yy + (1 - x), wide), f_recv.at[mat, r])
            shared(mat, 1, r)

    def local(mat, run):
        def copy(blocks):
            run(
                pltpu.make_async_copy(
                    taken(mat, group, blocks), landing(mat, core, me, blocks), own_sem.at[mat]
                )
            )

        sized(short(core, group), copy)

    pure_z = [r for r, (dy, dz) in enumerate(sides) if not dy and dz]
    cross = [r for r, (dy, dz) in enumerate(sides) if dy and dz]
    near = [0, 1]
    keep_proj = pltpu.make_async_copy(out_proj, proj, own_sem.at[3])

    last_block = (wide - 1) * LANES
    w1[core, :, last_block:span] = jnp.zeros((w1.shape[1], LANES), jnp.bfloat16)
    w1[core, :, span + last_block :] = jnp.zeros((w1.shape[1], LANES), jnp.bfloat16)
    tail = pl.ds(pl.multiple_of(core * span + last_block, LANES), LANES)
    w2[tail] = jnp.zeros((LANES, inner), jnp.bfloat16)

    with jax.named_scope("greet"):
        partners = [at(x, *target(r)) for r in range(1, 2 * deep)]
        partners += [x_place, at(*fellow(3), z), twin]
        greet(partners)
    send(0, *pure_z)
    for mat in range(3):
        local(mat, lambda copy: copy.start())
    keep_proj.start()

    with jax.named_scope("local"):
        tokens = queries.shape[0]
        heads = queries.shape[1] // HK
        blocks = tokens // SPAN
        raw = decay_pre[...]
        logdecay = (jnp.minimum(raw, 0.0) - jnp.log1p(jnp.exp(-jnp.abs(raw)))) / TAU
        row = lax.broadcasted_iota(jnp.int32, (tokens, tokens), 0)
        col = lax.broadcasted_iota(jnp.int32, (tokens, tokens), 1)
        tri = jnp.logical_and(row // SPAN == col // SPAN, col <= row).astype(jnp.float32)
        cumul = jnp.dot(
            tri, logdecay, precision=lax.Precision.HIGHEST, preferred_element_type=jnp.float32
        )
        lasts = [cumul[(n + 1) * SPAN - 1 : (n + 1) * SPAN] for n in range(blocks)]
        across = (((0,), (0,)), ((), ()))

        def column(line):
            return jnp.broadcast_to(line, (HK, HK)).T

        def spread(square):
            return jnp.concatenate([square] * (HV // HK), axis=1)

        for n in range(blocks):
            steps = slice(n * SPAN, (n + 1) * SPAN)
            faded = keys[steps].astype(jnp.float32) * jnp.exp(lasts[n] - cumul[steps])
            high = faded.astype(jnp.bfloat16)
            low = (faded - high.astype(jnp.float32)).astype(jnp.bfloat16)
            for h in range(heads):
                key = slice(h * HK, (h + 1) * HK)
                value = values[steps, h * HV : (h + 1) * HV]
                updates[n, h] = lax.dot_general(
                    high[:, key], value, across, preferred_element_type=jnp.float32
                ) + lax.dot_general(
                    low[:, key], value, across, preferred_element_type=jnp.float32
                )
                ends[n, h] = column(jnp.exp(lasts[n][:, key]))
        whole = jnp.exp(sum(lasts))
        for h in range(heads):
            state = updates[0, h]
            for n in range(1, blocks):
                state = spread(ends[n, h]) * state + updates[n, h]
            s_out[h] = state.astype(jnp.bfloat16)
            d_out[h] = jnp.broadcast_to(whole[:, h * HK : (h + 1) * HK], d_out.shape[1:])

    def to_plane(dp):
        xx, yy = fellow(dp)
        goal, slot = at(xx, yy, z), 2 * yy + xx
        return (
            remote(s_out.at[slot], s_in.at[place], p1_send.at[dp, 0], p1_recv.at[dp, 0], goal),
            remote(d_out.at[slot], d_in.at[place], p1_send.at[dp, 1], p1_recv.at[dp, 1], goal),
        )

    for dp in range(1, plane):
        for copy in to_plane(dp):
            copy.start()
    s_in[place] = s_out[place]
    d_in[place] = d_out[place]
    send(0, *near)

    with jax.named_scope("p1"):
        for dp in range(1, plane):
            for copy in to_plane(dp):
                copy.wait_recv()
    running = jnp.zeros((HK, HV), jnp.float32)
    line = jnp.ones((1, HK), jnp.float32)
    reach = []
    for i in range(plane):
        before[i] = running
        reach.append(line)
        own_decay = d_in[i][:1]
        running = spread(column(own_decay)) * running + s_in[i].astype(jnp.float32)
        line = line * own_decay
    t_out[...] = running.astype(jnp.bfloat16)
    dt_out[...] = jnp.broadcast_to(line, dt_out.shape)

    def to_later(zz):
        goal = at(x, y, zz)
        return (
            remote(t_out, t_in.at[z], p2_send.at[zz, 0], p2_recv.at[z, 0], goal),
            remote(dt_out, dt_in.at[z], p2_send.at[zz, 1], p2_recv.at[z, 1], goal),
        )

    for zz in range(1, deep):

        @pl.when(zz > z)
        def _():
            for copy in to_later(zz):
                copy.start()

    send(0, *cross)
    send(1, *pure_z)
    with jax.named_scope("gates1"):
        pass_on(0, *pure_z)
    total[...] = jnp.zeros(total.shape, jnp.float32)
    with jax.named_scope("p2"):
        for zz in range(deep - 1):

            @pl.when(zz < z)
            def _():
                came(t_in.at[zz], p2_recv.at[zz, 0])
                came(dt_in.at[zz], p2_recv.at[zz, 1])
                fade = spread(column(dt_in[zz][:1]))
                total[...] = fade * total[...] + t_in[zz].astype(jnp.float32)

    for i in range(plane):
        s_start[i] = (before[i] + spread(column(reach[i])) * total[...]).astype(jnp.bfloat16)

    def to_fellow(dp):
        xx, yy = fellow(dp)
        slot = 2 * yy + xx
        return remote(
            s_start.at[slot], start.at[place], p3_send.at[dp], p3_recv.at[dp], at(xx, yy, z)
        )

    for dp in range(1, plane):
        to_fellow(dp).start()
    start[place] = s_start[place]
    send(1, *near)
    with jax.named_scope("gates2"):
        pass_on(0, *near)
    with jax.named_scope("p3"):
        for dp in range(1, plane):
            to_fellow(dp).wait_recv()

    with jax.named_scope("mix"):
        for h in range(heads):
            thick = slice(h * HV, (h + 1) * HV)
            state = start[h].astype(jnp.float32)
            reads = []
            for n in range(blocks):
                state = spread(ends[n, h]) * state + updates[n, h]
                high = state.astype(jnp.bfloat16)
                low = (state - high.astype(jnp.float32)).astype(jnp.bfloat16)
                query = queries[n * SPAN : (n + 1) * SPAN, h * HK : (h + 1) * HK]
                reads.append(
                    jnp.dot(query, high, preferred_element_type=jnp.float32)
                    + jnp.dot(query, low, preferred_element_type=jnp.float32)
                )
            read = jnp.concatenate(reads, axis=0) * HK ** (-0.5)
            size = jnp.mean(read * read, axis=-1, keepdims=True)
            pre = out_gate[:, thick].astype(jnp.float32)
            normed = read * lax.rsqrt(size + RMS_EPS) * head_gain[...]
            gated[:, thick] = (normed * (pre * jax.nn.sigmoid(pre))).astype(jnp.bfloat16)
    keep_proj.wait()
    with jax.named_scope("proj"):
        summed_heads = jnp.dot(gated[...], proj[...], preferred_element_type=jnp.float32)
        mixed[...] = summed_heads.astype(jnp.bfloat16).reshape(2, own, inner)
    swap = remote(mixed.at[1 - core], mixed_in, m_sem.at[0], m_sem.at[1], twin)
    swap.start()
    with jax.named_scope("swap"):
        swap.wait()
    with jax.named_scope("ln"):
        added = mixed[core].astype(jnp.float32) + mixed_in[...].astype(jnp.float32)
        middle = ALPHA * resid[core].astype(jnp.float32) + added
        rows[y, z] = layer_norm(middle, mix_gain[...], mix_shift[...]).astype(jnp.bfloat16)

    def climb(zz):
        block = rows.at[y, zz]
        return remote(block, block, au_send.at[zz], az_recv.at[zz], above)

    def sink(zz):
        block = rows.at[y, zz]
        return remote(block, block, av_send.at[zz], az_recv.at[zz], below)

    def cross_y(zz):
        block = rows.at[y, zz]
        return remote(block, block, ay_send.at[zz], ay_recv.at[zz], y_place)

    @pl.when(z < deep - 1)
    def _():
        climb(z).start()

    @pl.when(z > 0)
    def _():
        sink(z).start()

    cross_y(z).start()
    send(1, *cross)
    send(2, *pure_z)

    def landed(far):
        @pl.when(z >= far)
        def _():
            came(rows.at[y, z - far], az_recv.at[z - far])

            @pl.when(z < deep - 1)
            def _():
                climb(z - far).start()

            cross_y(z - far).start()

        @pl.when(z < deep - far)
        def _():
            came(rows.at[y, z + far], az_recv.at[z + far])

            @pl.when(z > 0)
            def _():
                sink(z + far).start()

            cross_y(z + far).start()

    with jax.named_scope("wa"):
        for mat in range(3):
            local(mat, lambda copy: copy.wait())
        share(0, 0, 0).start()
        share(1, 0, 0).start()
        pass_on(0, *cross)
        pass_on(1, *near)
        pass_on(1, *pure_z)
    with jax.named_scope("ag1"):
        landed(1)
    send(2, *near)
    send(2, *cross)
    with jax.named_scope("wb"):
        passed(0, *range(1, 2 * deep))
    with jax.named_scope("ag2"):
        landed(2)
    with jax.named_scope("wc"):
        pass_on(1, *cross)
    with jax.named_scope("ag3"):
        for far in range(3, deep):
            landed(far)
    with jax.named_scope("wd"):
        pass_on(2, *near)
        pass_on(2, *pure_z)
        passed(1, *range(1, 2 * deep))
    with jax.named_scope("agy"):
        for zz in range(deep):
            came(rows.at[1 - y, zz], ay_recv.at[zz])
    with jax.named_scope("we"):
        for k in range(2):
            for r in range(2 * deep):
                yy, zz = origin(r)
                s = plane * zz + 2 * yy + (x + k) % 2
                came(slab(0, 1 - core, s), t_recv.at[0, k, r])

    def hide(side, slot):
        left = rows[side].reshape(deep * own, inner)
        for c in range(2):
            both = jnp.dot(left, w1[c], preferred_element_type=jnp.float32)
            gate, up = both[:, :span], both[:, span:]
            hidden[slot, :, c * span : (c + 1) * span] = (
                gate * jax.nn.sigmoid(gate) * up
            ).astype(jnp.bfloat16)

    def lower(side, slot):
        down = jnp.dot(hidden[slot], w2[...], preferred_element_type=jnp.float32)
        part[side] = down.astype(jnp.bfloat16).reshape(deep, own, inner)

    with jax.named_scope("hide0"):
        hide(1 - y, 0)
    with jax.named_scope("wf"):
        pass_on(2, *cross)
    with jax.named_scope("hide1"):
        hide(y, 1)
    with jax.named_scope("wg"):
        passed(2, *range(1, 2 * deep))
        for k in range(2):
            for r in range(2 * deep):
                yy, zz = origin(r)
                s = plane * zz + 2 * yy + (x + k) % 2
                came(slab(1, 1 - core, s), t_recv.at[1, k, r])

    low_side = z < deep // 2
    order = [
        jnp.where(low_side, deep - 1, 0),
        jnp.where(low_side, deep - 2, 1),
        jnp.where(low_side, 1 - z, 2 * deep - 3 - z),
        z,
    ]

    def across_y(d):
        return remote(part.at[1 - y, d], y_in.at[d], ry_send.at[d], ry_recv.at[d], y_place)

    def hop(i, up):
        d = order[i]
        into, sem = (u_in, ru_recv) if up else (v_in, rv_recv)
        return remote(z_out.at[i], into.at[d], rz_send.at[i], sem.at[d], above if up else below)

    with jax.named_scope("down0"):
        lower(1 - y, 0)
    for d in order:
        across_y(d).start()
    with jax.named_scope("down1"):
        lower(y, 1)

    def gather_in(d, from_below, from_above):
        came(y_in.at[d], ry_recv.at[d])
        acc[...] = part[y, d].astype(jnp.float32) + y_in[d].astype(jnp.float32)

        @pl.when(from_below)
        def _():
            came(u_in.at[d], ru_recv.at[d])
            acc[...] += u_in[d].astype(jnp.float32)

        @pl.when(from_above)
        def _():
            came(v_in.at[d], rv_recv.at[d])
            acc[...] += v_in[d].astype(jnp.float32)

    for i in range(deep - 1):
        with jax.named_scope(f"rs{i}"):
            d = order[i]
            up = d > z
            gather_in(
                d,
                jnp.logical_and(up, z > 0),
                jnp.logical_and(jnp.logical_not(up), z < deep - 1),
            )
            z_out[i] = acc[...].astype(jnp.bfloat16)

            @pl.when(up)
            def _():
                hop(i, True).start()

            @pl.when(jnp.logical_not(up))
            def _():
                hop(i, False).start()

    with jax.named_scope("rsend"):
        gather_in(z, z > 0, z < deep - 1)
    with jax.named_scope("fin"):
        finished = layer_norm(
            ALPHA * rows[y, z].astype(jnp.float32) + 0.5 * acc[...], gain[...], shift[...]
        )
        out[core] = finished.astype(jnp.bfloat16)
    last = remote(out.at[core], out.at[core], f_sem.at[0], f_sem.at[1], twin)
    last.start()

    with jax.named_scope("drain"):
        for mat in range(3):
            for r in range(2 * deep):
                bring(mat, r, lambda copy: copy.wait_send())
                if r:
                    relay(mat, r).wait_send()
        for j in range(2):
            for k in range(2):
                for r in range(2 * deep):
                    share(j, k, r).wait_send()
        for dp in range(1, plane):
            for copy in (*to_plane(dp), to_fellow(dp)):
                copy.wait_send()
        for zz in range(deep):

            @pl.when(zz > z)
            def _():
                for copy in to_later(zz):
                    copy.wait_send()

            @pl.when(jnp.logical_and(zz <= z, z < deep - 1))
            def _():
                climb(zz).wait_send()

            @pl.when(jnp.logical_and(zz >= z, z > 0))
            def _():
                sink(zz).wait_send()

            cross_y(zz).wait_send()
            across_y(zz).wait_send()
        for i in range(deep - 1):
            hop(i, True).wait_send()
        last.wait()


def layer(
    resid,
    queries,
    keys,
    values,
    decay_pre,
    out_gate,
    head_gain,
    out_proj,
    mix_gain,
    mix_shift,
    gate_in,
    up_in,
    down_out,
    gain,
    shift,
):
    count = lax.axis_size("sp")
    tok_rows, inner = resid.shape
    own = tok_rows // 2
    deep = count // 4
    groups = count // 2
    wide = -(-(gate_in.shape[1] // LANES) // groups)
    span = wide * LANES
    heads = queries.shape[1] // HK
    steps = tok_rows // SPAN
    dma = pltpu.SemaphoreType.DMA
    half, full = jnp.bfloat16, jnp.float32
    block = lambda *lead: pltpu.VMEM((*lead, own, inner), half)
    near, far = pl.BlockSpec(memory_space=pltpu.VMEM), pl.BlockSpec(memory_space=pl.ANY)
    out = pl.pallas_call(
        functools.partial(layer_kernel, deep, wide),
        out_shape=jax.ShapeDtypeStruct((2, own, inner), half),
        in_specs=[near] * 6 + [far] + [near] * 3 + [far] * 3 + [near] * 2,
        out_specs=near,
        scratch_shapes=[
            pltpu.VMEM((2, inner, 2 * span), half),
            pltpu.VMEM((2 * span, inner), half),
            pltpu.VMEM(out_proj.shape, half),
            pltpu.VMEM((steps, heads, HK, HV), full),
            pltpu.VMEM((steps, heads, HK, HK), full),
            pltpu.VMEM((heads, HK, HV), half),
            pltpu.VMEM((heads, 8, HK), full),
            pltpu.VMEM((4, HK, HV), half),
            pltpu.VMEM((4, 8, HK), full),
            pltpu.VMEM((4, HK, HV), full),
            pltpu.VMEM((HK, HV), full),
            pltpu.VMEM((HK, HV), half),
            pltpu.VMEM((deep, HK, HV), half),
            pltpu.VMEM((8, HK), full),
            pltpu.VMEM((deep, 8, HK), full),
            pltpu.VMEM((4, HK, HV), half),
            pltpu.VMEM((4, HK, HV), half),
            pltpu.VMEM((tok_rows, out_proj.shape[0]), half),
            block(2),
            block(),
            block(2, deep),
            pltpu.VMEM((2, deep * own, 2 * span), half),
            block(2, deep),
            block(deep),
            block(deep),
            block(deep),
            block(deep - 1),
            pltpu.VMEM((own, inner), full),
            dma((4,)),
            dma((3, groups)),
            dma((3, groups)),
            dma((3, groups)),
            dma((3, groups)),
            dma((2, 2, groups)),
            dma((2, 2, groups)),
            dma((4, 2)),
            dma((4, 2)),
            dma((deep, 2)),
            dma((deep, 2)),
            dma((4,)),
            dma((4,)),
            dma((2,)),
            dma((deep,)),
            dma((deep,)),
            dma((deep,)),
            dma((deep,)),
            dma((deep,)),
            dma((deep,)),
            dma((deep,)),
            dma((deep,)),
            dma((deep,)),
            dma((deep,)),
            dma((2,)),
        ],
        compiler_params=pltpu.CompilerParams(
            collective_id=2, has_side_effects=True, vmem_limit_bytes=60 * 1024 * 1024
        ),
    )(
        queries,
        keys,
        values,
        decay_pre,
        out_gate,
        head_gain[None],
        out_proj,
        resid.reshape(2, own, inner),
        mix_gain[None],
        mix_shift[None],
        gate_in,
        up_in,
        down_out,
        gain[None],
        shift[None],
    )
    return out.reshape(tok_rows, inner)


def body(
    resid,
    queries,
    keys,
    values,
    decay_pre,
    out_gate,
    head_gain,
    out_proj,
    mix_gain,
    mix_shift,
    gate_in,
    up_in,
    down_out,
    out_gain,
    out_shift,
):
    tp_count = lax.axis_size("tp")
    tok_rows = queries.shape[0]
    own_count = tok_rows // tp_count
    sp_count = lax.axis_size("sp")
    units = gate_in.shape[1]
    heads = queries.shape[1] // HK
    groups = sp_count // 2
    unit_blocks = units // LANES
    by_units = (
        tp_count == 2
        and sp_count == 16
        and heads == 4
        and units % LANES == 0
        and unit_blocks % groups == groups - 2
        and gate_in.shape[0] % LANES == 0
        and down_out.shape[1] % LANES == 0
        and gate_in.shape[0] * sp_count == resid.shape[1]
        and own_count % 16 == 0
        and tok_rows % SPAN == 0
    )
    if by_units:
        return layer(
            resid,
            queries,
            keys,
            values,
            decay_pre,
            out_gate,
            head_gain,
            out_proj,
            mix_gain,
            mix_shift,
            gate_in,
            up_in,
            down_out,
            out_gain,
            out_shift,
        )
    local = local_tokens(queries, keys, values, decay_pre)
    gated = mix_tokens(*local, out_gate, head_gain)
    mixed = lax.psum_scatter(
        jnp.dot(gated, out_proj, preferred_element_type=jnp.float32).astype(jnp.bfloat16),
        "tp",
        scatter_dimension=0,
        tiled=True,
    ).astype(jnp.float32)
    own_resid = lax.dynamic_slice_in_dim(resid, lax.axis_index("tp") * own_count, own_count, 0)
    mid = layer_norm(ALPHA * own_resid.astype(jnp.float32) + mixed, mix_gain, mix_shift).astype(
        jnp.bfloat16
    )
    whole_rows = lax.all_gather(mid, "tp", axis=0, tiled=True)
    hidden = hidden_by_rows(whole_rows, gate_in, up_in)
    ffn = lax.psum_scatter(
        down_by_columns(hidden, down_out).astype(jnp.bfloat16),
        "tp",
        scatter_dimension=0,
        tiled=True,
    ).astype(jnp.float32)
    finished = layer_norm(ALPHA * mid.astype(jnp.float32) + 0.5 * ffn, out_gain, out_shift).astype(
        jnp.bfloat16
    )
    return lax.all_gather(finished, "tp", axis=0, tiled=True)


def solution(mesh):
    return jax.shard_map(
        body,
        mesh=mesh,
        in_specs=(
            P("sp", None),
            P("sp", "tp"),
            P("sp", "tp"),
            P("sp", "tp"),
            P("sp", "tp"),
            P("sp", "tp"),
            P(),
            P("tp", None),
            P(),
            P(),
            P("sp", "tp"),
            P("sp", "tp"),
            P("tp", "sp"),
            P(),
            P(),
        ),
        out_specs=P("sp", None),
        check_vma=False,
    )
```

time: 174 us -> 131 us (0.75); the launches traced: 171 us -> 131 us
  Pallas kernels: 155 us -> 129 us
  local copies, waits for them, and re-layouts: 9.51 us -> 1.88 us
  other arithmetic: 4.89 us -> 0 us
    pallas_call x1, Pallas kernels: 155 us -> 129 us  [layer(): pl.pallas_call(functools.partial(layer_kernel, deep, wide), out_shape=jax...]
    concatenate x2 -> x0, other arithmetic: 2.38 us -> none  [the longest x1 1.5 us: own_units(): jnp.concatenate([gate_in.T.reshape(count, piece, inner), up_in.T.reshape(...]
    reshape x3 -> x0, local copies, waits for them, and re-layouts: 2.22 us -> none  [the longest x1 1.14 us: local_tokens(): values.astype(jnp.float32).reshape(blocks, SPAN, local_heads, HV)]
    unnamed x10 -> x1, local copies, waits for them, and re-layouts: 3.94 us -> 1.88 us
    dynamic_update_slice x2 -> x0, local copies, waits for them, and re-layouts: 1.76 us -> none  [local_tokens(): lax.scan(advance, jnp.zeros((local_heads, HK, HV), jnp.float32), (last, u...]
where the time goes in v1:
time: 131 us
  Pallas kernels  129 us (98%)
  local copies, waits for them, and re-layouts  1.88 us (1%)
    pallas_call x1, Pallas kernels, layer(): pl.pallas_call(functools.partial(layer_kernel, deep, wide), out_shape=jax...  129 us

profile of v1, /device:TPU:0, one launch (start us, length us, event | category | flops | bytes accessed | tf_op | source)
XLA Modules:
  0.0 130.9 jit_solution(12052980162303061337)
XLA Ops:
  0.0 129.0 %shard_map.145 = bf16[2,64,2048]{2,1,0:T(8,128)(2,1)} custom-call(bf16[128,512]{1,0:T(8,128)(2,1)} %queries.1, bf16[128,512]{1,0:T(8,128)(2,1)} %keys.1, bf16[128,1024]{1,0:T(8,128)(2,1)} %values.1, f32[128,512]{1,0:T(8,128)} %decay_pre.1, bf16[128,1024]{1,0:T(8,128)(2,1)} %out_gate.1, f32[1,256]{1,0:T(1,128)} %bitcast.13, bf16[1024,2048]{1,0:T(8,128)(2,1)} %out_proj.1, ...), custom_call_target="tpu_custom_call" | custom-call | tf_op jit(solution)/shard_map/pallas_call | solution.py:761
  129.0 1.9 %copy.17 = bf16[128,2048]{1,0:T(8,128)(2,1)} copy(bf16[128,2048]{1,0:T(8,128)(2,1)} %bitcast.7) | data formatting | bytes 1048576

commit v2 on v1

--- a/solution.py
+++ b/solution.py
@@ -173,8 +173,6 @@
     total,
     t_out,
     t_in,
-    dt_out,
-    dt_in,
     s_start,
     start,
     gated,
@@ -197,8 +195,7 @@
     t_recv,
     p1_send,
     p1_recv,
-    p2_send,
-    p2_recv,
+    p2_sem,
     p3_send,
     p3_recv,
     m_sem,
@@ -213,6 +210,7 @@
     ru_recv,
     rv_recv,
     f_sem,
+    go_sem,
 ):
     me, core = lax.axis_index("sp"), lax.axis_index("tp")
     x, y, z = me % 2, (me // 2) % 2, me // 4
@@ -230,16 +228,19 @@
     y_place = (me + 2 - 4 * y, core)
     above, below = (me + plane, core), (me - plane, core)
     sides = [(dy, dz) for dz in range(deep) for dy in range(2)]
+    bottom = z < deep // 2
+    edge = jnp.logical_or(z == 0, z == deep - 1)
+    pair = z + 1 - 2 * (z % 2)
+    inner_z = jnp.where(bottom, deep // 2, deep // 2 - 1)
+    edge_z = jnp.where(bottom, deep - 1, 0)
 
     def at(xx, yy, zz):
         return (plane * zz + 2 * yy + xx, core)
 
-    def target(r):
-        dy, dz = sides[r]
+    def target(dy, dz):
         return (y + dy) % 2, (z + dz) % deep
 
-    def origin(r):
-        dy, dz = sides[r]
+    def origin(dy, dz):
         return (y + dy) % 2, (z + deep - dz) % deep
 
     def fellow(dp):
@@ -276,10 +277,14 @@
             return w1.at[c, pl.ds(pl.multiple_of(s * depth, depth), depth)]
         return landing(2, c, s, wide)
 
-    def bring(mat, r, run):
-        yy, zz = target(r)
-        goal = at(x, yy, zz) if r else x_place
+    def home(dy, dz):
+        return isinstance(dz, int) and dy == 0 and dz == 0
+
+    def bring(mat, dy, dz, run):
+        yy, zz = target(dy, dz)
+        goal = x_place if home(dy, dz) else at(x, yy, zz)
         g = 2 * zz + yy
+        r = 2 * dz + dy
 
         def copy(blocks):
             run(
@@ -294,46 +299,76 @@
 
         sized(short(core, g), copy)
 
-    def send(mat, *which):
-        for r in which:
-            bring(mat, r, lambda copy: copy.start())
-
-    def relay(mat, r):
-        yy, zz = origin(r)
-        s = plane * zz + 2 * yy + x
-        block = landing(mat, core, s, wide)
-        return remote(block, block, f_send.at[mat, r], f_recv.at[mat, r], x_place)
-
-    def share(j, k, r):
-        yy, zz = origin(r)
-        s = plane * zz + 2 * yy + (x + k) % 2
-        block = slab(j, core, s)
+    def send(mat, dy, dz):
+        bring(mat, dy, dz, lambda copy: copy.start())
+
+    def send_near(mat):
+        send(mat, 0, 0)
+        send(mat, 1, 0)
+
+    def send_to(mat, dy, zz):
+        send(mat, dy, (zz + deep - z) % deep)
+
+    def source(dy, dz, k):
+        yy, zz = origin(dy, dz)
+        return plane * zz + 2 * yy + (x + k) % 2
+
+    def relay(mat, dy, dz, run):
+        r = 2 * dz + dy
+
+        def copy(blocks):
+            block = landing(mat, core, source(dy, dz, 0), blocks)
+            run(remote(block, block, f_send.at[mat, r], f_recv.at[mat, r], x_place))
+
+        sized(short(core, group), copy)
+
+    def share(j, k, dy, dz):
+        block = slab(j, core, source(dy, dz, k))
+        r = 2 * dz + dy
         return remote(block, block, t_send.at[j, k, r], t_recv.at[j, k, r], twin)
 
     def came(ref, sem):
-        remote(ref, ref, f_sem.at[0], sem, twin).wait_recv()
-
-    def shared(mat, k, r):
+        remote(ref, ref, f_sem.at[0, 0], sem, twin).wait_recv()
+
+    def shared(mat, k, dy, dz):
         if mat:
-            share(mat - 1, k, r).start()
-
-    def pass_on(mat, *which):
-        for r in which:
-            yy, zz = origin(r)
-            s = plane * zz + 2 * yy + x if r else x_place[0]
+            share(mat - 1, k, dy, dz).start()
+
+    def pass_on(mat, dy, dz):
+        k = 1 if home(dy, dz) else 0
+        sized(
+            short(core, group),
+            lambda blocks: came(
+                landing(mat, core, source(dy, dz, k), blocks), b_recv.at[mat, 2 * dz + dy]
+            ),
+        )
+        if not k:
+            relay(mat, dy, dz, lambda copy: copy.start())
+        shared(mat, k, dy, dz)
+
+    def pass_on_near(mat):
+        pass_on(mat, 0, 0)
+        pass_on(mat, 1, 0)
+
+    def pass_on_from(mat, dy, zz):
+        pass_on(mat, dy, (z + deep - zz) % deep)
+
+    def passed(mat, *levels):
+        def one(dy, dz):
             sized(
                 short(core, group),
-                lambda blocks, s=s, r=r: came(landing(mat, core, s, blocks), b_recv.at[mat, r]),
+                lambda blocks: came(
+                    landing(mat, core, source(dy, dz, 1), blocks), f_recv.at[mat, 2 * dz + dy]
+                ),
             )
-            if r:
-                relay(mat, r).start()
-            shared(mat, 0 if r else 1, r)
-
-    def passed(mat, *which):
-        for r in which:
-            yy, zz = origin(r)
-            came(landing(mat, core, plane * zz + 2 * yy + (1 - x), wide), f_recv.at[mat, r])
-            shared(mat, 1, r)
+            shared(mat, 1, dy, dz)
+
+        for zz in levels:
+            if zz is None:
+                one(1, 0)
+            else:
+                for dy in range(2):
+                    one(dy, (z + deep - zz) % deep)
 
     def local(mat, run):
         def copy(blocks):
@@ -345,9 +380,6 @@
 
         sized(short(core, group), copy)
 
-    pure_z = [r for r, (dy, dz) in enumerate(sides) if not dy and dz]
-    cross = [r for r, (dy, dz) in enumerate(sides) if dy and dz]
-    near = [0, 1]
     keep_proj = pltpu.make_async_copy(out_proj, proj, own_sem.at[3])
 
     last_block = (wide - 1) * LANES
@@ -357,10 +389,11 @@
     w2[tail] = jnp.zeros((LANES, inner), jnp.bfloat16)
 
     with jax.named_scope("greet"):
-        partners = [at(x, *target(r)) for r in range(1, 2 * deep)]
+        partners = [at(x, *target(dy, dz)) for dy, dz in sides[1:]]
         partners += [x_place, at(*fellow(3), z), twin]
         greet(partners)
-    send(0, *pure_z)
+    for zz in (inner_z, edge_z, pair):
+        send_to(0, 0, zz)
     for mat in range(3):
         local(mat, lambda copy: copy.start())
     keep_proj.start()
@@ -421,7 +454,7 @@
             copy.start()
     s_in[place] = s_out[place]
     d_in[place] = d_out[place]
-    send(0, *near)
+    send_near(0)
 
     with jax.named_scope("p1"):
         for dp in range(1, plane):
@@ -436,37 +469,34 @@
         own_decay = d_in[i][:1]
         running = spread(column(own_decay)) * running + s_in[i].astype(jnp.float32)
         line = line * own_decay
-    t_out[...] = running.astype(jnp.bfloat16)
-    dt_out[...] = jnp.broadcast_to(line, dt_out.shape)
-
-    def to_later(zz):
-        goal = at(x, y, zz)
-        return (
-            remote(t_out, t_in.at[z], p2_send.at[zz, 0], p2_recv.at[z, 0], goal),
-            remote(dt_out, dt_in.at[z], p2_send.at[zz, 1], p2_recv.at[z, 1], goal),
-        )
-
-    for zz in range(1, deep):
-
-        @pl.when(zz > z)
+    total[...] = jnp.zeros(total.shape, jnp.float32)
+
+    def to_next():
+        return remote(t_out, t_in, p2_sem.at[0], p2_sem.at[1], above)
+
+    def push_on():
+        t_out[...] = (spread(column(line)) * total[...] + running).astype(jnp.bfloat16)
+        to_next().start()
+
+    @pl.when(z == 0)
+    def _():
+        push_on()
+
+    @pl.when(jnp.logical_not(bottom))
+    def _():
+        for mat, dy, zz in ((1, 0, inner_z), (1, 0, edge_z), (0, 1, inner_z)):
+            send_to(mat, dy, zz)
+
+    with jax.named_scope("p2"):
+
+        @pl.when(z > 0)
         def _():
-            for copy in to_later(zz):
-                copy.start()
-
-    send(0, *cross)
-    send(1, *pure_z)
-    with jax.named_scope("gates1"):
-        pass_on(0, *pure_z)
-    total[...] = jnp.zeros(total.shape, jnp.float32)
-    with jax.named_scope("p2"):
-        for zz in range(deep - 1):
-
-            @pl.when(zz < z)
-            def _():
-                came(t_in.at[zz], p2_recv.at[zz, 0])
-                came(dt_in.at[zz], p2_recv.at[zz, 1])
-                fade = spread(column(dt_in[zz][:1]))
-                total[...] = fade * total[...] + t_in[zz].astype(jnp.float32)
+            came(t_in, p2_sem.at[1])
+            total[...] = t_in[...].astype(jnp.float32)
+
+    @pl.when(jnp.logical_and(z > 0, z < deep - 1))
+    def _():
+        push_on()
 
     for i in range(plane):
         s_start[i] = (before[i] + spread(column(reach[i])) * total[...]).astype(jnp.bfloat16)
@@ -481,9 +511,26 @@
     for dp in range(1, plane):
         to_fellow(dp).start()
     start[place] = s_start[place]
-    send(1, *near)
+    send_to(1, 0, pair)
+    send_to(2, 0, pair)
+    send_to(0, 1, pair)
+
+    @pl.when(bottom)
+    def _():
+        for zz in (inner_z, edge_z):
+            send_to(1, 0, zz)
+            send_to(0, 1, zz)
+
+    @pl.when(jnp.logical_not(bottom))
+    def _():
+        send_to(0, 1, edge_z)
+
+    send_near(1)
+    send_near(2)
     with jax.named_scope("gates2"):
-        pass_on(0, *near)
+        pass_on_near(0)
+        for zz in (pair, edge_z, inner_z):
+            pass_on_from(0, 0, zz)
     with jax.named_scope("p3"):
         for dp in range(1, plane):
             to_fellow(dp).wait_recv()
@@ -520,85 +567,134 @@
         middle = ALPHA * resid[core].astype(jnp.float32) + added
         rows[y, z] = layer_norm(middle, mix_gain[...], mix_shift[...]).astype(jnp.bfloat16)
 
-    def climb(zz):
-        block = rows.at[y, zz]
-        return remote(block, block, au_send.at[zz], az_recv.at[zz], above)
-
-    def sink(zz):
-        block = rows.at[y, zz]
-        return remote(block, block, av_send.at[zz], az_recv.at[zz], below)
-
-    def cross_y(zz):
-        block = rows.at[y, zz]
-        return remote(block, block, ay_send.at[zz], ay_recv.at[zz], y_place)
-
-    @pl.when(z < deep - 1)
-    def _():
-        climb(z).start()
-
-    @pl.when(z > 0)
-    def _():
-        sink(z).start()
-
-    cross_y(z).start()
-    send(1, *cross)
-    send(2, *pure_z)
+    halves = range(2)
+    chunk = own // 2
+    bit = [pl.ds(h * chunk, chunk) for h in halves]
+
+    def climb(zz, h):
+        block = rows.at[y, zz, bit[h]]
+        return remote(block, block, au_send.at[zz, h], az_recv.at[zz, h], above)
+
+    def sink(zz, h):
+        block = rows.at[y, zz, bit[h]]
+        return remote(block, block, av_send.at[zz, h], az_recv.at[zz, h], below)
+
+    def cross_y(zz, h):
+        block = rows.at[y, zz, bit[h]]
+        return remote(block, block, ay_send.at[zz, h], ay_recv.at[zz, h], y_place)
+
+    for h in halves:
+
+        @pl.when(z < deep - 1)
+        def _():
+            climb(z, h).start()
+
+        @pl.when(z > 0)
+        def _():
+            sink(z, h).start()
+
+        cross_y(z, h).start()
 
     def landed(far):
-        @pl.when(z >= far)
-        def _():
-            came(rows.at[y, z - far], az_recv.at[z - far])
-
-            @pl.when(z < deep - 1)
+        for h in halves:
+
+            @pl.when(z >= far)
             def _():
-                climb(z - far).start()
-
-            cross_y(z - far).start()
-
-        @pl.when(z < deep - far)
-        def _():
-            came(rows.at[y, z + far], az_recv.at[z + far])
-
-            @pl.when(z > 0)
+                came(rows.at[y, z - far, bit[h]], az_recv.at[z - far, h])
+
+                @pl.when(z < deep - 1)
+                def _():
+                    climb(z - far, h).start()
+
+                cross_y(z - far, h).start()
+
+            @pl.when(z < deep - far)
             def _():
-                sink(z + far).start()
-
-            cross_y(z + far).start()
+                came(rows.at[y, z + far, bit[h]], az_recv.at[z + far, h])
+
+                @pl.when(z > 0)
+                def _():
+                    sink(z + far, h).start()
+
+                cross_y(z + far, h).start()
 
     with jax.named_scope("wa"):
         for mat in range(3):
             local(mat, lambda copy: copy.wait())
-        share(0, 0, 0).start()
-        share(1, 0, 0).start()
-        pass_on(0, *cross)
-        pass_on(1, *near)
-        pass_on(1, *pure_z)
+        share(0, 0, 0, 0).start()
+        share(1, 0, 0, 0).start()
+        pass_on_near(1)
+        for zz in (pair, edge_z, inner_z):
+            pass_on_from(1, 0, zz)
+        pass_on_from(0, 1, pair)
+        pass_on_from(2, 0, pair)
     with jax.named_scope("ag1"):
         landed(1)
-    send(2, *near)
-    send(2, *cross)
+
+    send_to(1, 1, pair)
+    send_to(2, 1, pair)
+
+    def second_wave():
+        for zz in (inner_z, edge_z):
+            send_to(1, 1, zz)
+        for dy in range(2):
+            for zz in (inner_z, edge_z):
+                send_to(2, dy, zz)
+
+    @pl.when(jnp.logical_not(edge))
+    def _():
+        second_wave()
+
     with jax.named_scope("wb"):
-        passed(0, *range(1, 2 * deep))
+        for zz in (edge_z, inner_z):
+            pass_on_from(0, 1, zz)
+        pass_on_near(2)
     with jax.named_scope("ag2"):
         landed(2)
+
+    @pl.when(jnp.logical_not(edge))
+    def _():
+        pl.semaphore_signal(
+            go_sem, inc=1, device_id=at(x, y, edge_z), device_id_type=MESH
+        )
+
+    with jax.named_scope("go"):
+
+        @pl.when(edge)
+        def _():
+            pl.semaphore_wait(go_sem, 1)
+            second_wave()
+
     with jax.named_scope("wc"):
-        pass_on(1, *cross)
+        pass_on_from(1, 1, pair)
     with jax.named_scope("ag3"):
         for far in range(3, deep):
             landed(far)
     with jax.named_scope("wd"):
-        pass_on(2, *near)
-        pass_on(2, *pure_z)
-        passed(1, *range(1, 2 * deep))
+        pass_on_from(1, 1, inner_z)
+        pass_on_from(1, 1, edge_z)
+        pass_on_from(2, 1, pair)
+        pass_on_from(2, 0, edge_z)
+        pass_on_from(2, 0, inner_z)
+    with jax.named_scope("we"):
+        pass_on_from(2, 1, edge_z)
+        pass_on_from(2, 1, inner_z)
+    with jax.named_scope("wf"):
+        passed(0, None, pair, edge_z, inner_z)
+        passed(1, None, pair, edge_z, inner_z)
     with jax.named_scope("agy"):
         for zz in range(deep):
-            came(rows.at[1 - y, zz], ay_recv.at[zz])
-    with jax.named_scope("we"):
-        for k in range(2):
-            for r in range(2 * deep):
-                yy, zz = origin(r)
-                s = plane * zz + 2 * yy + (x + k) % 2
-                came(slab(0, 1 - core, s), t_recv.at[0, k, r])
+            for h in halves:
+                came(rows.at[1 - y, zz, bit[h]], ay_recv.at[zz, h])
+    def twins(j, *levels):
+        for zz in levels:
+            dz = 0 if zz is None else (z + deep - zz) % deep
+            for k in range(2):
+                for dy in range(2):
+                    came(slab(j, 1 - core, source(dy, dz, k)), t_recv.at[j, k, 2 * dz + dy])
+
+    with jax.named_scope("wt"):
+        twins(0, None, pair, edge_z, inner_z)
 
     def hide(side, slot):
         left = rows[side].reshape(deep * own, inner)
@@ -609,122 +705,151 @@
                 gate * jax.nn.sigmoid(gate) * up
             ).astype(jnp.bfloat16)
 
-    def lower(side, slot):
-        down = jnp.dot(hidden[slot], w2[...], preferred_element_type=jnp.float32)
-        part[side] = down.astype(jnp.bfloat16).reshape(deep, own, inner)
+    wing = inner // 2
+    early = jnp.where(bottom, 0, 1)
+    late = 1 - early
+    columns = lambda h: pl.ds(pl.multiple_of(h * wing, wing), wing)
+
+    def lower(side, slot, h):
+        down = jnp.dot(hidden[slot], w2[:, columns(h)], preferred_element_type=jnp.float32)
+        part[side, :, :, columns(h)] = down.astype(jnp.bfloat16).reshape(deep, own, wing)
+
+    order = [
+        jnp.where(bottom, deep - 1, 0),
+        jnp.where(bottom, deep - 2, 1),
+        jnp.where(bottom, 1 - z, 2 * deep - 3 - z),
+        z,
+    ]
+
+    def across_y(d, h):
+        return remote(
+            part.at[1 - y, d, :, columns(h)],
+            y_in.at[d, :, columns(h)],
+            ry_send.at[d, h],
+            ry_recv.at[d, h],
+            y_place,
+        )
+
+    def hop(i, h, up):
+        into, sem = (u_in, ru_recv) if up else (v_in, rv_recv)
+        return remote(
+            z_out.at[i, :, columns(h)],
+            into.at[order[i], :, columns(h)],
+            rz_send.at[i, h],
+            sem.at[order[i], h],
+            above if up else below,
+        )
+
+    def gather_in(d, h, from_below, from_above):
+        taken = columns(h)
+        came(y_in.at[d, :, taken], ry_recv.at[d, h])
+        acc[:, taken] = part[y, d, :, taken].astype(jnp.float32) + y_in[d, :, taken].astype(
+            jnp.float32
+        )
+
+        @pl.when(from_below)
+        def _():
+            came(u_in.at[d, :, taken], ru_recv.at[d, h])
+            acc[:, taken] += u_in[d, :, taken].astype(jnp.float32)
+
+        @pl.when(from_above)
+        def _():
+            came(v_in.at[d, :, taken], rv_recv.at[d, h])
+            acc[:, taken] += v_in[d, :, taken].astype(jnp.float32)
+
+    def step(i, h):
+        d = order[i]
+        up = d > z
+        gather_in(
+            d,
+            h,
+            jnp.logical_and(up, z > 0),
+            jnp.logical_and(jnp.logical_not(up), z < deep - 1),
+        )
+        z_out[i, :, columns(h)] = acc[:, columns(h)].astype(jnp.bfloat16)
+
+        @pl.when(up)
+        def _():
+            hop(i, h, True).start()
+
+        @pl.when(jnp.logical_not(up))
+        def _():
+            hop(i, h, False).start()
 
     with jax.named_scope("hide0"):
         hide(1 - y, 0)
-    with jax.named_scope("wf"):
-        pass_on(2, *cross)
+    with jax.named_scope("wg"):
+        passed(2, None, pair)
+        twins(1, None, pair)
+    with jax.named_scope("down0"):
+        lower(1 - y, 0, early)
+    for d in order[:2]:
+        across_y(d, early).start()
     with jax.named_scope("hide1"):
         hide(y, 1)
-    with jax.named_scope("wg"):
-        passed(2, *range(1, 2 * deep))
-        for k in range(2):
-            for r in range(2 * deep):
-                yy, zz = origin(r)
-                s = plane * zz + 2 * yy + (x + k) % 2
-                came(slab(1, 1 - core, s), t_recv.at[1, k, r])
-
-    low_side = z < deep // 2
-    order = [
-        jnp.where(low_side, deep - 1, 0),
-        jnp.where(low_side, deep - 2, 1),
-        jnp.where(low_side, 1 - z, 2 * deep - 3 - z),
-        z,
-    ]
-
-    def across_y(d):
-        return remote(part.at[1 - y, d], y_in.at[d], ry_send.at[d], ry_recv.at[d], y_place)
-
-    def hop(i, up):
-        d = order[i]
-        into, sem = (u_in, ru_recv) if up else (v_in, rv_recv)
-        return remote(z_out.at[i], into.at[d], rz_send.at[i], sem.at[d], above if up else below)
-
-    with jax.named_scope("down0"):
-        lower(1 - y, 0)
-    for d in order:
-        across_y(d).start()
     with jax.named_scope("down1"):
-        lower(y, 1)
-
-    def gather_in(d, from_below, from_above):
-        came(y_in.at[d], ry_recv.at[d])
-        acc[...] = part[y, d].astype(jnp.float32) + y_in[d].astype(jnp.float32)
-
-        @pl.when(from_below)
-        def _():
-            came(u_in.at[d], ru_recv.at[d])
-            acc[...] += u_in[d].astype(jnp.float32)
-
-        @pl.when(from_above)
-        def _():
-            came(v_in.at[d], rv_recv.at[d])
-            acc[...] += v_in[d].astype(jnp.float32)
-
-    for i in range(deep - 1):
-        with jax.named_scope(f"rs{i}"):
-            d = order[i]
-            up = d > z
-            gather_in(
-                d,
-                jnp.logical_and(up, z > 0),
-                jnp.logical_and(jnp.logical_not(up), z < deep - 1),
-            )
-            z_out[i] = acc[...].astype(jnp.bfloat16)
-
-            @pl.when(up)
-            def _():
-                hop(i, True).start()
-
-            @pl.when(jnp.logical_not(up))
-            def _():
-                hop(i, False).start()
-
-    with jax.named_scope("rsend"):
-        gather_in(z, z > 0, z < deep - 1)
+        lower(y, 1, early)
+    with jax.named_scope("wh"):
+        passed(2, edge_z, inner_z)
+        twins(1, edge_z, inner_z)
+    with jax.named_scope("down2"):
+        lower(1 - y, 0, late)
+    for d in order[:2]:
+        across_y(d, late).start()
+    for d in order[2:]:
+        for h in (early, late):
+            across_y(d, h).start()
+    with jax.named_scope("down3"):
+        lower(y, 1, late)
+    for i, h in ((0, early), (1, early), (0, late), (1, late), (2, early), (2, late)):
+        with jax.named_scope("rs%d%d" % (i, h is late)):
+            step(i, h)
+    with jax.named_scope("rsend0"):
+        gather_in(z, early, z > 0, z < deep - 1)
+    with jax.named_scope("rsend1"):
+        gather_in(z, late, z > 0, z < deep - 1)
     with jax.named_scope("fin"):
         finished = layer_norm(
             ALPHA * rows[y, z].astype(jnp.float32) + 0.5 * acc[...], gain[...], shift[...]
         )
         out[core] = finished.astype(jnp.bfloat16)
-    last = remote(out.at[core], out.at[core], f_sem.at[0], f_sem.at[1], twin)
+    last = remote(out.at[core], out.at[core], f_sem.at[0, 0], f_sem.at[1, 0], twin)
     last.start()
 
     with jax.named_scope("drain"):
-        for mat in range(3):
-            for r in range(2 * deep):
-                bring(mat, r, lambda copy: copy.wait_send())
-                if r:
-                    relay(mat, r).wait_send()
-        for j in range(2):
-            for k in range(2):
-                for r in range(2 * deep):
-                    share(j, k, r).wait_send()
+
+        @pl.when(z < deep - 1)
+        def _():
+            to_next().wait_send()
+
+        for dy, dz in sides:
+            for mat in range(3):
+                bring(mat, dy, dz, lambda copy: copy.wait_send())
+                if (dy, dz) != (0, 0):
+                    relay(mat, dy, dz, lambda copy: copy.wait_send())
+            for j in range(2):
+                for k in range(2):
+                    share(j, k, dy, dz).wait_send()
         for dp in range(1, plane):
             for copy in (*to_plane(dp), to_fellow(dp)):
                 copy.wait_send()
         for zz in range(deep):
 
-            @pl.when(zz > z)
-            def _():
-                for copy in to_later(zz):
-                    copy.wait_send()
-
-            @pl.when(jnp.logical_and(zz <= z, z < deep - 1))
-            def _():
-                climb(zz).wait_send()
-
-            @pl.when(jnp.logical_and(zz >= z, z > 0))
-            def _():
-                sink(zz).wait_send()
-
-            cross_y(zz).wait_send()
-            across_y(zz).wait_send()
-        for i in range(deep - 1):
-            hop(i, True).wait_send()
+            for h in halves:
+
+                @pl.when(jnp.logical_and(zz <= z, z < deep - 1))
+                def _():
+                    climb(zz, h).wait_send()
+
+                @pl.when(jnp.logical_and(zz >= z, z > 0))
+                def _():
+                    sink(zz, h).wait_send()
+
+                cross_y(zz, h).wait_send()
+                across_y(zz, h).wait_send()
+        for h in halves:
+            for i in range(deep - 1):
+                hop(i, h, True).wait_send()
         last.wait()
 
 
@@ -776,9 +901,7 @@
             pltpu.VMEM((4, HK, HV), full),
             pltpu.VMEM((HK, HV), full),
             pltpu.VMEM((HK, HV), half),
-            pltpu.VMEM((deep, HK, HV), half),
-            pltpu.VMEM((8, HK), full),
-            pltpu.VMEM((deep, 8, HK), full),
+            pltpu.VMEM((HK, HV), half),
             pltpu.VMEM((4, HK, HV), half),
             pltpu.VMEM((4, HK, HV), half),
             pltpu.VMEM((tok_rows, out_proj.shape[0]), half),
@@ -801,22 +924,13 @@
             dma((2, 2, groups)),
             dma((4, 2)),
             dma((4, 2)),
-            dma((deep, 2)),
-            dma((deep, 2)),
+            dma((2,)),
             dma((4,)),
             dma((4,)),
             dma((2,)),
-            dma((deep,)),
-            dma((deep,)),
-            dma((deep,)),
-            dma((deep,)),
-            dma((deep,)),
-            dma((deep,)),
-            dma((deep,)),
-            dma((deep,)),
-            dma((deep,)),
-            dma((deep,)),
-            dma((2,)),
+            *[dma((deep, 2))] * 10,
+            dma((2, 2)),
+            pltpu.SemaphoreType.REGULAR,
         ],
         compiler_params=pltpu.CompilerParams(
             collective_id=2, has_side_effects=True, vmem_limit_bytes=60 * 1024 * 1024

time: 131 us -> 113 us (0.86)
  Pallas kernels: 129 us -> 111 us
    pallas_call x1, Pallas kernels: 129 us -> 111 us  [layer(): pl.pallas_call(functools.partial(layer_kernel, deep, wide), out_shape=jax...]
where the time goes in v2:
time: 113 us; the launch traced here: 112 us
  Pallas kernels  111 us (98%)
  local copies, waits for them, and re-layouts  1.88 us (2%)
    pallas_call x1, Pallas kernels, layer(): pl.pallas_call(functools.partial(layer_kernel, deep, wide), out_shape=jax...  111 us

profile of v2, /device:TPU:0, one launch (start us, length us, event | category | flops | bytes accessed | tf_op | source)
XLA Modules:
  0.0 112.4 jit_solution(4578467181037394820)
XLA Ops:
  0.0 110.6 %shard_map.145 = bf16[2,64,2048]{2,1,0:T(8,128)(2,1)} custom-call(bf16[128,512]{1,0:T(8,128)(2,1)} %queries.1, bf16[128,512]{1,0:T(8,128)(2,1)} %keys.1, bf16[128,1024]{1,0:T(8,128)(2,1)} %values.1, f32[128,512]{1,0:T(8,128)} %decay_pre.1, bf16[128,1024]{1,0:T(8,128)(2,1)} %out_gate.1, f32[1,256]{1,0:T(1,128)} %bitcast.13, bf16[1024,2048]{1,0:T(8,128)(2,1)} %out_proj.1, ...), custom_call_target="tpu_custom_call" | custom-call | tf_op jit(solution)/shard_map/pallas_call | solution.py:886
  110.6 1.9 %copy.17 = bf16[128,2048]{1,0:T(8,128)(2,1)} copy(bf16[128,2048]{1,0:T(8,128)(2,1)} %bitcast.7) | data formatting | bytes 1048576

commit v3 on v2

--- a/solution.py
+++ b/solution.py
@@ -144,14 +144,14 @@
 def layer_kernel(
     deep,
     wide,
-    queries,
-    keys,
-    values,
-    decay_pre,
-    out_gate,
+    queries_far,
+    keys_far,
+    values_far,
+    decay_pre_far,
+    out_gate_far,
     head_gain,
     out_proj,
-    resid,
+    resid_far,
     mix_gain,
     mix_shift,
     gate_in,
@@ -160,6 +160,12 @@
     gain,
     shift,
     out,
+    queries,
+    keys,
+    values,
+    decay_pre,
+    out_gate,
+    resid,
     w1,
     w2,
     proj,
@@ -211,6 +217,7 @@
     rv_recv,
     f_sem,
     go_sem,
+    near_sem,
 ):
     me, core = lax.axis_index("sp"), lax.axis_index("tp")
     x, y, z = me % 2, (me // 2) % 2, me // 4
@@ -382,11 +389,21 @@
 
     keep_proj = pltpu.make_async_copy(out_proj, proj, own_sem.at[3])
 
-    last_block = (wide - 1) * LANES
-    w1[core, :, last_block:span] = jnp.zeros((w1.shape[1], LANES), jnp.bfloat16)
-    w1[core, :, span + last_block :] = jnp.zeros((w1.shape[1], LANES), jnp.bfloat16)
-    tail = pl.ds(pl.multiple_of(core * span + last_block, LANES), LANES)
-    w2[tail] = jnp.zeros((LANES, inner), jnp.bfloat16)
+    keep_near = [
+        pltpu.make_async_copy(ref, copy, near_sem.at[i])
+        for i, (ref, copy) in enumerate(
+            (
+                (decay_pre_far, decay_pre),
+                (keys_far, keys),
+                (values_far, values),
+                (queries_far, queries),
+                (out_gate_far, out_gate),
+                (resid_far, resid),
+            )
+        )
+    ]
+    for copy in keep_near:
+        copy.start()
 
     with jax.named_scope("greet"):
         partners = [at(x, *target(dy, dz)) for dy, dz in sides[1:]]
@@ -399,6 +416,8 @@
     keep_proj.start()
 
     with jax.named_scope("local"):
+        for copy in keep_near[:3]:
+            copy.wait()
         tokens = queries.shape[0]
         heads = queries.shape[1] // HK
         blocks = tokens // SPAN
@@ -456,6 +475,15 @@
     d_in[place] = d_out[place]
     send_near(0)
 
+    @pl.when(short(core, group))
+    def _():
+        last_block = (wide - 1) * LANES
+        blank = jnp.zeros((w1.shape[1], LANES), jnp.bfloat16)
+        w1[core, :, last_block:span] = blank
+        w1[core, :, span + last_block :] = blank
+        tail = pl.ds(pl.multiple_of(core * span + last_block, LANES), LANES)
+        w2[tail] = jnp.zeros((LANES, inner), jnp.bfloat16)
+
     with jax.named_scope("p1"):
         for dp in range(1, plane):
             for copy in to_plane(dp):
@@ -487,6 +515,17 @@
         for mat, dy, zz in ((1, 0, inner_z), (1, 0, edge_z), (0, 1, inner_z)):
             send_to(mat, dy, zz)
 
+    def gates():
+        pass_on_near(0)
+        for zz in (pair, edge_z, inner_z):
+            pass_on_from(0, 0, zz)
+
+    with jax.named_scope("gates1"):
+
+        @pl.when(jnp.logical_not(bottom))
+        def _():
+            gates()
+
     with jax.named_scope("p2"):
 
         @pl.when(z > 0)
@@ -528,14 +567,18 @@
     send_near(1)
     send_near(2)
     with jax.named_scope("gates2"):
-        pass_on_near(0)
-        for zz in (pair, edge_z, inner_z):
-            pass_on_from(0, 0, zz)
+
+        @pl.when(bottom)
+        def _():
+            gates()
+
     with jax.named_scope("p3"):
         for dp in range(1, plane):
             to_fellow(dp).wait_recv()
 
     with jax.named_scope("mix"):
+        for copy in keep_near[3:]:
+            copy.wait()
         for h in range(heads):
             thick = slice(h * HV, (h + 1) * HV)
             state = start[h].astype(jnp.float32)
@@ -595,6 +638,13 @@
 
         cross_y(z, h).start()
 
+    ahead = jnp.logical_not(jnp.logical_or(bottom, edge))
+
+    @pl.when(ahead)
+    def _():
+        for zz in (inner_z, edge_z):
+            send_to(1, 1, zz)
+
     def landed(far):
         for h in halves:
 
@@ -635,8 +685,11 @@
     send_to(2, 1, pair)
 
     def second_wave():
-        for zz in (inner_z, edge_z):
-            send_to(1, 1, zz)
+        @pl.when(jnp.logical_not(ahead))
+        def _():
+            for zz in (inner_z, edge_z):
+                send_to(1, 1, zz)
+
         for dy in range(2):
             for zz in (inner_z, edge_z):
                 send_to(2, dy, zz)
@@ -885,10 +938,16 @@
     near, far = pl.BlockSpec(memory_space=pltpu.VMEM), pl.BlockSpec(memory_space=pl.ANY)
     out = pl.pallas_call(
         functools.partial(layer_kernel, deep, wide),
-        out_shape=jax.ShapeDtypeStruct((2, own, inner), half),
-        in_specs=[near] * 6 + [far] + [near] * 3 + [far] * 3 + [near] * 2,
+        out_shape=pltpu.VMEM((2, own, inner), half),
+        in_specs=[far] * 5 + [near] + [far] * 2 + [near] * 2 + [far] * 3 + [near] * 2,
         out_specs=near,
         scratch_shapes=[
+            pltpu.VMEM(queries.shape, half),
+            pltpu.VMEM(keys.shape, half),
+            pltpu.VMEM(values.shape, half),
+            pltpu.VMEM(decay_pre.shape, full),
+            pltpu.VMEM(out_gate.shape, half),
+            block(2),
             pltpu.VMEM((2, inner, 2 * span), half),
             pltpu.VMEM((2 * span, inner), half),
             pltpu.VMEM(out_proj.shape, half),
@@ -931,6 +990,7 @@
             *[dma((deep, 2))] * 10,
             dma((2, 2)),
             pltpu.SemaphoreType.REGULAR,
+            dma((6,)),
         ],
         compiler_params=pltpu.CompilerParams(
             collective_id=2, has_side_effects=True, vmem_limit_bytes=60 * 1024 * 1024

time: 113 us -> 108 us (0.956)
  Pallas kernels: 111 us -> 107 us
    pallas_call x1, Pallas kernels: 111 us -> 107 us  [layer(): pl.pallas_call(functools.partial(layer_kernel, deep, wide), out_shape=plt...]
where the time goes in v3:
time: 108 us; the launch traced here: 107 us
  Pallas kernels  107 us (99%)
    pallas_call x1, Pallas kernels, layer(): pl.pallas_call(functools.partial(layer_kernel, deep, wide), out_shape=plt...  107 us

profile of v3, /device:TPU:0, one launch (start us, length us, event | category | flops | bytes accessed | tf_op | source)
XLA Modules:
  0.0 107.4 jit_solution(6376102045389072900)
XLA Ops:
  0.0 106.6 %shard_map.145 = bf16[2,64,2048]{2,1,0:T(8,128)(2,1)S(1)} custom-call(bf16[128,512]{1,0:T(8,128)(2,1)} %queries_far.1, bf16[128,512]{1,0:T(8,128)(2,1)} %keys_far.1, bf16[128,1024]{1,0:T(8,128)(2,1)} %values_far.1, f32[128,512]{1,0:T(8,128)} %decay_pre_far.1, bf16[128,1024]{1,0:T(8,128)(2,1)} %out_gate_far.1, f32[1,256]{1,0:T(1,128)} %bitcast.13, ...), custom_call_target="tpu_custom_call" | custom-call | tf_op jit(solution)/shard_map/pallas_call | solution.py:939
  106.6 0.8 copy.17

commit v4 on v3

--- a/solution.py
+++ b/solution.py
@@ -711,6 +711,10 @@
             go_sem, inc=1, device_id=at(x, y, edge_z), device_id_type=MESH
         )
 
+    with jax.named_scope("wc"):
+        pass_on_from(1, 1, pair)
+        pass_on_from(2, 1, pair)
+
     with jax.named_scope("go"):
 
         @pl.when(edge)
@@ -718,23 +722,30 @@
             pl.semaphore_wait(go_sem, 1)
             second_wave()
 
-    with jax.named_scope("wc"):
-        pass_on_from(1, 1, pair)
     with jax.named_scope("ag3"):
         for far in range(3, deep):
             landed(far)
+    with jax.named_scope("wd0"):
+        passed(0, None, pair, edge_z, inner_z)
+        passed(1, None, pair)
     with jax.named_scope("wd"):
         pass_on_from(1, 1, inner_z)
         pass_on_from(1, 1, edge_z)
-        pass_on_from(2, 1, pair)
+        passed(2, None, pair)
         pass_on_from(2, 0, edge_z)
         pass_on_from(2, 0, inner_z)
-    with jax.named_scope("we"):
+    def last_blocks():
         pass_on_from(2, 1, edge_z)
         pass_on_from(2, 1, inner_z)
+
+    with jax.named_scope("we"):
+
+        @pl.when(jnp.logical_not(bottom))
+        def _():
+            last_blocks()
+
     with jax.named_scope("wf"):
-        passed(0, None, pair, edge_z, inner_z)
-        passed(1, None, pair, edge_z, inner_z)
+        passed(1, edge_z, inner_z)
     with jax.named_scope("agy"):
         for zz in range(deep):
             for h in halves:
@@ -774,10 +785,14 @@
         z,
     ]
 
+    slim = wing // 2
+    columns_of = lambda q: pl.ds(pl.multiple_of(q * slim, slim), slim)
+    quarters = lambda h: (2 * h, 2 * h + 1)
+
     def across_y(d, h):
         return remote(
-            part.at[1 - y, d, :, columns(h)],
-            y_in.at[d, :, columns(h)],
+            part.at[1 - y, d, :, columns_of(h)],
+            y_in.at[d, :, columns_of(h)],
             ry_send.at[d, h],
             ry_recv.at[d, h],
             y_place,
@@ -786,15 +801,15 @@
     def hop(i, h, up):
         into, sem = (u_in, ru_recv) if up else (v_in, rv_recv)
         return remote(
-            z_out.at[i, :, columns(h)],
-            into.at[order[i], :, columns(h)],
+            z_out.at[i, :, columns_of(h)],
+            into.at[order[i], :, columns_of(h)],
             rz_send.at[i, h],
             sem.at[order[i], h],
             above if up else below,
         )
 
     def gather_in(d, h, from_below, from_above):
-        taken = columns(h)
+        taken = columns_of(h)
         came(y_in.at[d, :, taken], ry_recv.at[d, h])
         acc[:, taken] = part[y, d, :, taken].astype(jnp.float32) + y_in[d, :, taken].astype(
             jnp.float32
@@ -819,7 +834,7 @@
             jnp.logical_and(up, z > 0),
             jnp.logical_and(jnp.logical_not(up), z < deep - 1),
         )
-        z_out[i, :, columns(h)] = acc[:, columns(h)].astype(jnp.bfloat16)
+        z_out[i, :, columns_of(h)] = acc[:, columns_of(h)].astype(jnp.bfloat16)
 
         @pl.when(up)
         def _():
@@ -831,13 +846,19 @@
 
     with jax.named_scope("hide0"):
         hide(1 - y, 0)
+    with jax.named_scope("wx"):
+
+        @pl.when(bottom)
+        def _():
+            last_blocks()
+
     with jax.named_scope("wg"):
-        passed(2, None, pair)
         twins(1, None, pair)
     with jax.named_scope("down0"):
         lower(1 - y, 0, early)
     for d in order[:2]:
-        across_y(d, early).start()
+        for q in quarters(early):
+            across_y(d, q).start()
     with jax.named_scope("hide1"):
         hide(y, 1)
     with jax.named_scope("down1"):
@@ -848,19 +869,24 @@
     with jax.named_scope("down2"):
         lower(1 - y, 0, late)
     for d in order[:2]:
-        across_y(d, late).start()
+        for q in quarters(late):
+            across_y(d, q).start()
     for d in order[2:]:
         for h in (early, late):
-            across_y(d, h).start()
+            for q in quarters(h):
+                across_y(d, q).start()
     with jax.named_scope("down3"):
         lower(y, 1, late)
     for i, h in ((0, early), (1, early), (0, late), (1, late), (2, early), (2, late)):
         with jax.named_scope("rs%d%d" % (i, h is late)):
-            step(i, h)
+            for q in quarters(h):
+                step(i, q)
     with jax.named_scope("rsend0"):
-        gather_in(z, early, z > 0, z < deep - 1)
+        for q in quarters(early):
+            gather_in(z, q, z > 0, z < deep - 1)
     with jax.named_scope("rsend1"):
-        gather_in(z, late, z > 0, z < deep - 1)
+        for q in quarters(late):
+            gather_in(z, q, z > 0, z < deep - 1)
     with jax.named_scope("fin"):
         finished = layer_norm(
             ALPHA * rows[y, z].astype(jnp.float32) + 0.5 * acc[...], gain[...], shift[...]
@@ -899,10 +925,11 @@
                     sink(zz, h).wait_send()
 
                 cross_y(zz, h).wait_send()
-                across_y(zz, h).wait_send()
-        for h in halves:
+        for q in range(4):
+            for i in range(deep):
+                across_y(i, q).wait_send()
             for i in range(deep - 1):
-                hop(i, h, True).wait_send()
+                hop(i, q, True).wait_send()
         last.wait()
 
 
@@ -987,7 +1014,8 @@
             dma((4,)),
             dma((4,)),
             dma((2,)),
-            *[dma((deep, 2))] * 10,
+            *[dma((deep, 2))] * 5,
+            *[dma((deep, 4))] * 5,
             dma((2, 2)),
             pltpu.SemaphoreType.REGULAR,
             dma((6,)),

time: 108 us -> 104 us (0.963)
  Pallas kernels: 107 us -> 103 us
    pallas_call x1, Pallas kernels: 107 us -> 103 us  [layer(): pl.pallas_call(functools.partial(layer_kernel, deep, wide), out_shape=plt...]
where the time goes in v4:
time: 104 us
  Pallas kernels  103 us (99%)
    pallas_call x1, Pallas kernels, layer(): pl.pallas_call(functools.partial(layer_kernel, deep, wide), out_shape=plt...  103 us

profile of v4, /device:TPU:0, one launch (start us, length us, event | category | flops | bytes accessed | tf_op | source)
XLA Modules:
  0.0 104.2 jit_solution(12522082393002416878)
XLA Ops:
  0.0 103.4 %shard_map.145 = bf16[2,64,2048]{2,1,0:T(8,128)(2,1)S(1)} custom-call(bf16[128,512]{1,0:T(8,128)(2,1)} %queries_far.1, bf16[128,512]{1,0:T(8,128)(2,1)} %keys_far.1, bf16[128,1024]{1,0:T(8,128)(2,1)} %values_far.1, f32[128,512]{1,0:T(8,128)} %decay_pre_far.1, bf16[128,1024]{1,0:T(8,128)(2,1)} %out_gate_far.1, f32[1,256]{1,0:T(1,128)} %bitcast.13, ...), custom_call_target="tpu_custom_call" | custom-call | tf_op jit(solution)/shard_map/pallas_call | solution.py:966
  103.4 0.8 copy.17

commit v5 on v4

--- a/solution.py
+++ b/solution.py
@@ -785,9 +785,9 @@
         z,
     ]
 
-    slim = wing // 2
+    slim = wing // 4
     columns_of = lambda q: pl.ds(pl.multiple_of(q * slim, slim), slim)
-    quarters = lambda h: (2 * h, 2 * h + 1)
+    pieces = lambda h: [4 * h + i for i in range(4)]
 
     def across_y(d, h):
         return remote(
@@ -857,7 +857,7 @@
     with jax.named_scope("down0"):
         lower(1 - y, 0, early)
     for d in order[:2]:
-        for q in quarters(early):
+        for q in pieces(early):
             across_y(d, q).start()
     with jax.named_scope("hide1"):
         hide(y, 1)
@@ -869,23 +869,23 @@
     with jax.named_scope("down2"):
         lower(1 - y, 0, late)
     for d in order[:2]:
-        for q in quarters(late):
+        for q in pieces(late):
             across_y(d, q).start()
     for d in order[2:]:
         for h in (early, late):
-            for q in quarters(h):
+            for q in pieces(h):
                 across_y(d, q).start()
     with jax.named_scope("down3"):
         lower(y, 1, late)
     for i, h in ((0, early), (1, early), (0, late), (1, late), (2, early), (2, late)):
         with jax.named_scope("rs%d%d" % (i, h is late)):
-            for q in quarters(h):
+            for q in pieces(h):
                 step(i, q)
     with jax.named_scope("rsend0"):
-        for q in quarters(early):
+        for q in pieces(early):
             gather_in(z, q, z > 0, z < deep - 1)
     with jax.named_scope("rsend1"):
-        for q in quarters(late):
+        for q in pieces(late):
             gather_in(z, q, z > 0, z < deep - 1)
     with jax.named_scope("fin"):
         finished = layer_norm(
@@ -925,7 +925,7 @@
                     sink(zz, h).wait_send()
 
                 cross_y(zz, h).wait_send()
-        for q in range(4):
+        for q in range(8):
             for i in range(deep):
                 across_y(i, q).wait_send()
             for i in range(deep - 1):
@@ -1015,7 +1015,7 @@
             dma((4,)),
             dma((2,)),
             *[dma((deep, 2))] * 5,
-            *[dma((deep, 4))] * 5,
+            *[dma((deep, 8))] * 5,
             dma((2, 2)),
             pltpu.SemaphoreType.REGULAR,
             dma((6,)),

time: 104 us -> 104 us (level)
  no operation moved by 1% of the time
where the time goes in v5:
time: 104 us; the launch traced here: 103 us
  Pallas kernels  103 us (99%)
    pallas_call x1, Pallas kernels, layer(): pl.pallas_call(functools.partial(layer_kernel, deep, wide), out_shape=plt...  103 us

profile of v5, /device:TPU:0, one launch (start us, length us, event | category | flops | bytes accessed | tf_op | source)
XLA Modules:
  0.0 103.5 jit_solution(8122267056814771233)
XLA Ops:
  0.0 102.7 %shard_map.145 = bf16[2,64,2048]{2,1,0:T(8,128)(2,1)S(1)} custom-call(bf16[128,512]{1,0:T(8,128)(2,1)} %queries_far.1, bf16[128,512]{1,0:T(8,128)(2,1)} %keys_far.1, bf16[128,1024]{1,0:T(8,128)(2,1)} %values_far.1, f32[128,512]{1,0:T(8,128)} %decay_pre_far.1, bf16[128,1024]{1,0:T(8,128)(2,1)} %out_gate_far.1, f32[1,256]{1,0:T(1,128)} %bitcast.13, ...), custom_call_target="tpu_custom_call" | custom-call | tf_op jit(solution)/shard_map/pallas_call | solution.py:966
  102.7 0.8 copy.17
